TPU v7x, 32 devices: a whole 2x2x4 slice. The times are simulated.
32 devices in a mesh: sp: 4 (over z), fs: 4 (over y, x), tp: 2 (over core).
Axes of the slice: x: 2, y: 2, z: 4, core: 2. Of those that a mesh axis runs over, the one named last changes fastest.
Arguments:
- tokens: bfloat16 [4, 1024, 2048], P('fs', 'sp', 'tp'), may hold values from -6 to 6
- norm_gain: float32 [2048], replicated, may hold values from 0.1 to 1.9
- ret_query: bfloat16 [2048, 1024], P('sp', 'tp'), may hold values from -0.125 to 0.125
- ret_key: bfloat16 [2048, 1024], P('sp', 'tp'), may hold values from -0.125 to 0.125
- ret_value: bfloat16 [2048, 1024], P('sp', 'tp'), may hold values from -0.125 to 0.125
- att_query: bfloat16 [2048, 1024], P('sp', 'tp'), may hold values from -0.125 to 0.125
- att_key: bfloat16 [2048, 256], P('sp', 'tp'), may hold values from -0.125 to 0.125
- att_value: bfloat16 [2048, 256], P('sp', 'tp'), may hold values from -0.125 to 0.125
- log_decay: float32 [4, 4, 1024], P('fs', 'tp', 'sp'), may hold values from -1 to 0
- start_state: float32 [4, 4, 256, 256], P('fs', 'tp'), may hold values from -12 to 12
- ret_gain: float32 [1024], P('tp'), may hold values from 0.1 to 1.9
- sink_logits: float32 [16], P('tp'), may hold values from 1 to 5
- ret_out: bfloat16 [1024, 2048], P('tp', 'fs'), may hold values from -0.1875 to 0.1875
- att_out: bfloat16 [1024, 2048], P('tp', 'fs'), may hold values from -1.5 to 1.5
Outputs:
- mixed: bfloat16 [4, 1024, 2048], P('fs', 'sp', 'tp')
All inputs are finite; a program needn't handle non-finite values.
Results may differ from a plain program's by a relative error of at most 0.015.
Values may be sent and summed in bfloat16 or wider, within the bound.
A program may use at most 128 MiB of HBM per device.

v0:
```python
import functools

import jax
import jax.numpy as jnp
import numpy as np
from jax import lax
from jax.experimental import pallas as pl
from jax.experimental.pallas import tpu as pltpu
from jax.sharding import PartitionSpec as P

DK = 256
DV = 256
HD = 64
WINDOW = 128
BLOCK = 128


epsilon = 1e-06
exact_result = lax.Precision.HIGHEST


def carried_in(array, axis, combine, identity):
    peers, mine = (lax.axis_size(axis), lax.axis_index(axis))
    everything = jax.tree.map(
        lambda part, kind: lax.all_gather(part.astype(kind), axis),
        array,
        (jnp.bfloat16, jnp.bfloat16),
    )
    start = jax.tree.map(
        lambda part, zero: jnp.broadcast_to(jnp.asarray(zero, part.dtype), part.shape),
        array,
        identity,
    )

    def hop(k, before):
        reached = k < mine
        new = combine(
            before, jax.tree.map(lambda part, own: part[k].astype(own.dtype), everything, array)
        )
        return jax.tree.map(lambda a, b: jnp.where(reached, a, b), new, before)

    return lax.fori_loop(0, peers, hop, start)


def passed_along(block, axis, distance):
    devices = range(lax.axis_size(axis))
    route = [(i - distance, i) for i in devices if i - distance in devices]
    return lax.ppermute(block, axis, route)


def rotate(values, positions):
    half_dim = values.shape[-1] // 2
    inverse = 1.0 / 10000.0 ** (jnp.arange(half_dim, dtype=jnp.float32) / half_dim)
    angles = positions.astype(jnp.float32)[:, None] * inverse[None, :]
    cosine = jnp.cos(angles)[:, None, :]
    sine_table = jnp.sin(angles)[:, None, :]
    front_half = values[..., :half_dim]
    back_half = values[..., half_dim:]
    return jnp.concatenate(
        [
            front_half * cosine - back_half * sine_table,
            front_half * sine_table + back_half * cosine,
        ],
        axis=-1,
    )


def block_step(memory_state, inputs):
    queries, key_matrix_rows, value_matrix_rows, log_rates = inputs
    length_here = log_rates.shape[-1]
    causal = jnp.arange(length_here)[:, None] >= jnp.arange(length_here)[None, :]
    running_totals = jnp.cumsum(log_rates, axis=-1)
    relative = running_totals[:, :, None] - running_totals[:, None, :]
    weight = jnp.where(causal[None], jnp.exp(jnp.where(causal[None], relative, 0.0)), 0.0)
    score_matrix = (
        jnp.einsum("hqd,hkd->hqk", queries, key_matrix_rows, precision=exact_result) * weight
    )
    carried_state = jnp.einsum(
        "hqd,hdv->hqv",
        queries * jnp.exp(running_totals)[:, :, None],
        memory_state,
        precision=exact_result,
    )
    output_rows = (
        jnp.einsum("arf,afu->aru", score_matrix, value_matrix_rows, precision=exact_result)
        + carried_state
    )
    decay_factors = jnp.exp(running_totals[:, -1:] - running_totals)
    memory_state = memory_state * jnp.exp(running_totals[:, -1])[:, None, None] + jnp.einsum(
        "iwj,iwe->ije",
        key_matrix_rows * decay_factors[:, :, None],
        value_matrix_rows,
        precision=exact_result,
    )
    return (memory_state, output_rows)


def chain(earlier, later):
    return (earlier[0] * later[0], earlier[1] * later[0][:, None, None] + later[1])


def shards(
    tokens,
    norm_gain,
    ret_query,
    ret_key,
    ret_value,
    att_query,
    att_key,
    att_value,
    log_decay,
    start_state,
    ret_gain,
    sink_logits,
    ret_out,
    att_out,
):
    gathered = lax.all_gather(tokens[0], "tp", axis=1, tiled=True)
    row_count = gathered.shape[0]
    as_float = gathered.astype(jnp.float32)
    normed = (
        as_float
        * lax.rsqrt(jnp.mean(as_float * as_float, axis=-1, keepdims=True) + epsilon)
        * norm_gain
    ).astype(jnp.bfloat16)
    offset = lax.axis_index("sp") * row_count
    positions = offset + jnp.arange(row_count, dtype=jnp.int32)
    weights = (ret_query, ret_key, ret_value, att_query, att_key, att_value)
    pieces = (
        lax.all_gather(weights[0], "sp", axis=0, tiled=True),
        lax.all_gather(weights[1], "sp", axis=0, tiled=True),
        lax.all_gather(weights[2], "sp", axis=0, tiled=True),
        lax.all_gather(weights[3], "sp", axis=0, tiled=True),
        lax.all_gather(weights[4], "sp", axis=0, tiled=True),
        lax.all_gather(weights[5], "sp", axis=0, tiled=True),
    )
    projected = tuple(
        (jnp.dot(normed, piece, preferred_element_type=jnp.float32) for piece in pieces)
    )
    rounded = tuple((product_f.astype(jnp.bfloat16) for product_f in projected))
    projected = rounded[:3]
    head_count = projected[0].shape[1] // DK
    queries = rotate(projected[0].astype(jnp.float32).reshape(row_count, head_count, DK), positions)
    keys_rot = rotate(
        projected[1].astype(jnp.float32).reshape(row_count, head_count, DK), positions
    ) * DK ** (-0.5)
    values_f = projected[2].astype(jnp.float32).reshape(row_count, head_count, DV)
    log_rates = log_decay[0]
    count = row_count // BLOCK

    def blocked(array):
        return array.reshape(count, BLOCK, head_count, array.shape[-1]).transpose(0, 2, 1, 3)

    rates_blocked = log_rates.reshape(head_count, count, BLOCK).transpose(1, 0, 2)
    local_state, pieces = lax.scan(
        block_step,
        jnp.zeros((head_count, DK, DV), jnp.float32),
        (blocked(queries), blocked(keys_rot), blocked(values_f), rates_blocked),
    )
    local_out = pieces.transpose(0, 2, 1, 3).reshape(row_count, head_count, DV)
    running_totals = jnp.cumsum(log_rates, axis=-1)
    device_decay = jnp.exp(running_totals[:, -1])
    identity = (jnp.ones((head_count,), jnp.float32), jnp.zeros((head_count, DK, DV), jnp.float32))
    prior_decay, prior_state = carried_in((device_decay, local_state), "sp", chain, identity)
    incoming = prior_state + prior_decay[:, None, None] * start_state[0]
    retained = local_out + jnp.einsum(
        "thd,hdv->thv",
        queries * jnp.exp(running_totals).T[:, :, None],
        incoming,
        precision=exact_result,
    )
    centred = retained - jnp.mean(retained, axis=-1, keepdims=True)
    variance = jnp.mean(centred * centred, axis=-1, keepdims=True)
    ret_hidden = (
        (centred * lax.rsqrt(variance + epsilon)).reshape(row_count, head_count * DV) * ret_gain
    ).astype(jnp.bfloat16)
    att_queries, att_keys, att_values = rounded[3:]
    kv_heads = att_keys.shape[1] // HD
    groups = att_queries.shape[1] // HD // kv_heads
    earlier_keys, earlier_values = passed_along(
        (att_keys[row_count - WINDOW :], att_values[row_count - WINDOW :]), "sp", 1
    )
    extended_keys = jnp.concatenate([earlier_keys, att_keys], axis=0)
    extended_values = jnp.concatenate([earlier_values, att_values], axis=0)
    windows = row_count // WINDOW

    def banded(array):
        earlier = array[:row_count].reshape(windows, WINDOW, kv_heads, HD)
        current = array[WINDOW:].reshape(windows, WINDOW, kv_heads, HD)
        return jnp.concatenate([earlier, current], axis=1)

    key_band = banded(extended_keys)
    value_band = banded(extended_values)
    grouped_q = att_queries.reshape(windows, WINDOW, kv_heads, groups, HD)
    score_matrix = jnp.einsum(
        "nqhgd,nkhd->nhgqk", grouped_q, key_band, preferred_element_type=jnp.float32
    ) * HD ** (-0.5)
    query_index = WINDOW + jnp.arange(WINDOW)
    key_index = jnp.arange(2 * WINDOW)
    allowed = (key_index[None, :] <= query_index[:, None]) & (
        query_index[:, None] - key_index[None, :] < WINDOW
    )
    key_place = offset - WINDOW + jnp.arange(windows)[:, None] * WINDOW + key_index[None, :]
    visible = (allowed[None] & (key_place >= 0)[:, None, :])[:, None, None]
    expo = jnp.exp(jnp.where(visible, score_matrix, -1e30))
    summed = jnp.sum(expo, axis=-1, keepdims=True) + jnp.exp(sink_logits).reshape(
        1, kv_heads, groups, 1, 1
    )
    probs = (expo / summed).astype(jnp.bfloat16)
    attended = jnp.einsum(
        "nhgqk,nkhd->nqhgd", probs, value_band, preferred_element_type=jnp.float32
    )
    att_hidden = attended.astype(jnp.bfloat16).reshape(row_count, kv_heads * groups * HD)
    ret_width = ret_hidden.shape[1]
    joined = jnp.concatenate([ret_hidden, att_hidden], axis=1)[None]
    piece = lax.all_gather(joined, "fs", axis=0, tiled=True)
    product = jnp.einsum(
        "srh,hd->srd", piece[:, :, :ret_width], ret_out, preferred_element_type=jnp.float32
    )
    product = product + jnp.einsum(
        "srh,hd->srd", piece[:, :, ret_width:], att_out, preferred_element_type=jnp.float32
    )
    partial_rows = product.astype(jnp.bfloat16)
    regrouped = lax.all_to_all(partial_rows, "fs", split_axis=0, concat_axis=2, tiled=True)
    mixed = lax.psum_scatter(
        regrouped[0].astype(jnp.float32).astype(jnp.bfloat16), "tp", scatter_dimension=1, tiled=True
    )
    return mixed[None]


MESH = pl.DeviceIdType.MESH
F32 = jnp.float32
BF16 = jnp.bfloat16
GAIN_ROW = 0
DECAY_ROW = 1
SINK_ROW = 8


def dot(a, b):
    return jnp.dot(a, b, preferred_element_type=F32)


def dot_t(a, b):
    return lax.dot_general(a, b, (((1,), (1,)), ((), ())), preferred_element_type=F32)


def dot_l(a, b):
    return lax.dot_general(a, b, (((0,), (0,)), ((), ())), preferred_element_type=F32)


def fused(
    n_sp, n_fs, tok_in, ngain_in, rq, rk, rv, aq, ak, av, gain_in, decay_in, sink_in, start, ro, ao, cos_in, sin_in, out,
    tok, ngain, small, cos, sin, gain_v, decay_v, sink_v, insem,
    toks, ss_mine, ss_peer, w, wo, sm, s0, proj, kv, hid, hin, state, total,
    send, wsem, wpsem, smsem, ssem, sssem, tsem, osem, hsem, lsem,
):
    z, f, c = lax.axis_index("sp"), lax.axis_index("fs"), lax.axis_index("tp")
    peer = 1 - c
    inputs = [
        pltpu.make_async_copy(src, dst, insem.at[i])
        for i, (src, dst) in enumerate(
            ((tok_in, tok), (ngain_in, ngain), (gain_in, gain_v), (decay_in, decay_v),
             (sink_in, sink_v), (cos_in, cos), (sin_in, sin))
        )
    ]
    for copy in inputs:
        copy.start()
    rows, half = tok.shape
    depth = rq.shape[0]
    quarter = depth // n_fs
    heads_core = rq.shape[1] // DK
    kvw = ak.shape[1]
    groups = aq.shape[1] // kvw
    qw = groups * HD
    ret_cols, att_cols = 3 * DK, qw + 2 * kvw
    sub = lax.rem(z, heads_core)
    is0, is1 = c == 0, c == 1

    barrier = pltpu.get_barrier_semaphore()
    count = 0

    def greet(**where):
        pl.semaphore_signal(barrier, inc=1, device_id=where, device_id_type=MESH)

    greet(tp=peer)
    for t in range(2):
        for i in range(1, n_sp):
            greet(sp=lax.rem(z + i, n_sp), tp=jnp.int32(t))
            count += 1
        for i in range(1, n_fs):
            greet(fs=lax.rem(f + i, n_fs), tp=jnp.int32(t))
            count += 1
    pl.semaphore_wait(barrier, count + 1)

    sent = []
    slots = iter(range(send.shape[0]))

    def both(a, b):
        if a is None:
            return b
        return a if b is None else jnp.logical_and(a, b)

    def remote(cond, src, dst, rsem, slot=None, **where):
        slot = next(slots) if slot is None else slot
        copy = pltpu.make_async_remote_copy(
            src_ref=src, dst_ref=dst, send_sem=send.at[slot], recv_sem=rsem,
            device_id=where, device_id_type=MESH,
        )
        sent.append((cond, copy))
        if cond is None:
            copy.start()
        else:
            pl.when(cond)(copy.start)

    def local(cond, src, dst, sem):
        pl.when(cond)(pltpu.make_async_copy(src, dst, sem).start)

    def arrived(dst, sem):
        pltpu.make_async_copy(dst, dst, sem).wait()

    def wrows(at, n):
        return pl.ds(pl.multiple_of(at, quarter), n)

    for copy in inputs[2:5]:
        copy.wait()
    small[...] = jnp.zeros_like(small)
    small[pl.ds(GAIN_ROW, 1), pl.ds(0, gain_v.shape[1])] = gain_v[...]
    for j in range(heads_core):
        small[pl.ds(DECAY_ROW, 1), pl.ds(j * rows, rows)] = decay_v[pl.ds(j, 1), :]
    n_sink = sink_v.shape[1]
    diagonal = lax.broadcasted_iota(jnp.int32, (n_sink, n_sink), 0) == lax.broadcasted_iota(
        jnp.int32, (n_sink, n_sink), 1
    )
    column = jnp.sum(jnp.where(diagonal, sink_v[...], 0.0), axis=1, keepdims=True)
    small[pl.ds(SINK_ROW, n_sink), :] = jnp.broadcast_to(column, (n_sink, small.shape[1]))

    def pieces(j, kind):
        if kind == 0:
            return [(a, pl.ds(j * DK, DK), pl.ds(i * DK, DK)) for i, a in enumerate((rq, rk, rv))]
        return [
            (aq, pl.ds(j * qw, qw), pl.ds(0, qw)),
            (ak, pl.ds(0, kvw), pl.ds(qw, kvw)),
            (av, pl.ds(0, kvw), pl.ds(qw + kvw, kvw)),
        ]

    mine = pl.ds(pl.multiple_of(f * quarter, quarter), quarter)
    for j in range(heads_core):
        p = heads_core * c + j
        away = p != z
        here = p == z
        decay = small.at[pl.ds(0, SINK_ROW)], sm.at[z, pl.ds(0, SINK_ROW)]
        remote(away, *decay, smsem.at[z], sp=p, tp=jnp.int32(0))
        for kind in range(2):
            for i, (a, cs, cd) in enumerate(pieces(j, kind)):
                remote(
                    away, a.at[mine, cs], w.at[wrows(z * depth + f * quarter, quarter), cd],
                    wsem.at[z, i], sp=p, tp=jnp.int32(kind),
                )
        remote(here, small, sm.at[z], smsem.at[z], tp=peer)
        local(here, small, sm.at[z], smsem.at[z])
        for kind in range(2):
            same, other = both(here, c == kind), both(here, c != kind)
            for i, (a, cs, cd) in enumerate(pieces(j, kind)):
                dst = w.at[wrows(z * depth, depth), cd]
                local(same, a.at[:, cs], dst, wsem.at[z, i])
                remote(other, a.at[:, cs], dst, wsem.at[z, i], tp=peer)
        local(both(here, is0), start.at[j], s0, ssem)
        remote(both(here, is1), start.at[j], s0, ssem, tp=peer)

    fs_core = n_fs // 2
    owner = f // fs_core
    out_rows, out_cols = ro.shape

    def out_block(kind, core, fsrc):
        j = lax.rem(fsrc, fs_core)
        block = wo.at[kind, pl.ds(pl.multiple_of(core * out_rows, out_rows), out_rows),
                      pl.ds(pl.multiple_of(j * out_cols, out_cols), out_cols)]
        return block, osem.at[kind, core, j]

    beside, across = f + 1 - 2 * lax.rem(f, 2), lax.rem(f + 2, n_fs)
    corner = lax.rem(beside + 2, n_fs)

    def send_out(kind):
        a = (ro, ao)[kind]
        dst, sem = out_block(kind, c, f)
        remote(None, a, dst, sem, fs=beside, tp=owner)
        remote(None, a, dst, sem, fs=across, tp=owner)
        local(c == owner, a, dst, sem)
        remote(c != owner, a, dst, sem, tp=peer)

    def pass_out(kind):
        cond, fsrc, to = ((c == owner, beside, across), (c != owner, across, beside))[kind]
        for core in range(2):
            block, sem = out_block(kind, core, fsrc)
            pl.when(cond)(functools.partial(arrived, block, sem))
            remote(cond, block, block, sem, fs=to)

    send_out(0)
    send_out(1)

    inputs[0].wait()
    inputs[1].wait()
    x = tok[...].astype(F32)
    sq = x * x
    part = sq[:, :128]
    for i in range(1, half // 128):
        part = part + sq[:, i * 128 : (i + 1) * 128]
    ss_mine[...] = part
    remote(None, ss_mine, ss_peer, sssem, tp=peer)
    arrived(ss_peer, sssem)
    mean = jnp.sum(ss_mine[...] + ss_peer[...], axis=-1, keepdims=True) / (2 * half)
    scale = lax.rsqrt(mean + epsilon)
    g = ngain[:, pl.ds(pl.multiple_of(c * half, 128), half)]
    toks[z, c] = (tok[...].astype(F32) * scale * g).astype(BF16)

    def spread(zs, cond, up, down):
        block = toks.at[zs, c]
        if up is not None:
            remote(both(cond, up), block, block, tsem.at[zs, c], sp=lax.rem(z + 1, n_sp))
        if down is not None:
            remote(both(cond, down), block, block, tsem.at[zs, c], sp=lax.rem(z + n_sp - 1, n_sp))
        remote(cond, block, block, tsem.at[zs, c], tp=peer)

    spread(z, None, z < n_sp - 1, z > 0)

    def widths(act):
        for kind, cols in ((0, ret_cols), (1, att_cols)):
            act(c == kind, pl.ds(0, cols))

    for i in range(1, n_sp):
        zs = lax.rem(jnp.where(z < n_sp // 2, z + i, z + n_sp - i), n_sp)
        at = wrows(zs * depth + f * quarter, quarter)
        for kind in range(2):
            @pl.when(c == kind)
            def _():
                for n, (_, _, cd) in enumerate(pieces(0, kind)):
                    arrived(w.at[at, cd], wsem.at[zs, n])
        base = [next(slots) for _ in range(n_fs - 1)]
        for kind, cols in ((0, ret_cols), (1, att_cols)):
            for k in range(1, n_fs):
                block = w.at[at, pl.ds(0, cols)]
                remote(c == kind, block, block, wpsem.at[zs, f], slot=base[k - 1],
                       fs=lax.rem(f + k, n_fs))

    kv[pl.ds(0, WINDOW), :] = jnp.zeros((WINDOW, kv.shape[1]), BF16)

    def project(zs):
        at = pl.ds(pl.multiple_of(zs * rows, rows), rows)

        def tile(cols):
            return dot(toks[zs, 0], w[pl.ds(0, half), cols]) + dot(toks[zs, 1], w[pl.ds(half, half), cols])

        @pl.when(is0)
        def _():
            @pl.loop(0, 3)
            def _(i):
                cols = pl.ds(pl.multiple_of(i * DK, DK), DK)
                proj[at, cols] = tile(cols).astype(BF16)

            co, si = cos[at, :], sin[at, :]
            h = DK // 2
            for i, factor in ((0, 1.0), (1, DK ** (-0.5))):
                a = proj[at, pl.ds(i * DK, h)].astype(F32)
                b = proj[at, pl.ds(i * DK + h, h)].astype(F32)
                proj[at, pl.ds(i * DK, h)] = ((a * co - b * si) * factor).astype(BF16)
                proj[at, pl.ds(i * DK + h, h)] = ((a * si + b * co) * factor).astype(BF16)

        @pl.when(is1)
        def _():
            proj[at, pl.ds(0, qw)] = tile(pl.ds(0, qw)).astype(BF16)
            both_kv = tile(pl.ds(qw, 2 * kvw))
            to = pl.ds(pl.multiple_of(WINDOW + zs * rows, WINDOW), rows)
            for n in range(2):
                got = both_kv[:, n * kvw : n * kvw + HD]
                for s in range(1, heads_core):
                    got = jnp.where(sub == s, both_kv[:, n * kvw + s * HD : n * kvw + (s + 1) * HD], got)
                kv[to, pl.ds(n * 128, HD)] = got.astype(BF16)

    lane = lax.broadcasted_iota(jnp.int32, (BLOCK, BLOCK), 1)
    row = lax.broadcasted_iota(jnp.int32, (BLOCK, BLOCK), 0)
    per = rows // BLOCK

    def retention(p, i):
        b = p * per + i
        at = pl.ds(pl.multiple_of(b * BLOCK, BLOCK), BLOCK)
        l = sm[p, pl.ds(DECAY_ROW, 1), pl.ds(pl.multiple_of(sub * rows + i * BLOCK, BLOCK), BLOCK)]
        cum = jnp.sum(jnp.where(lane <= row, l, 0.0), axis=1, keepdims=True)
        cum_row = jnp.sum(jnp.where(lane == row, cum, 0.0), axis=0, keepdims=True)
        total = jnp.sum(l, axis=1, keepdims=True)
        weight = jnp.where(lane <= row, jnp.exp(jnp.where(lane <= row, cum - cum_row, 0.0)), 0.0)
        q, k, v = (proj[at, pl.ds(n * DK, DK)] for n in range(3))
        st = state[...]
        scores = (dot_t(q, k) * weight).astype(BF16)
        o = dot(scores, v) + dot((q.astype(F32) * jnp.exp(cum)).astype(BF16), st.astype(BF16))
        kd = (k.astype(F32) * jnp.exp(total - cum)).astype(BF16)
        state[...] = st * jnp.exp(total) + dot_l(kd, v)
        centred = o - jnp.mean(o, axis=-1, keepdims=True)
        var = jnp.mean(centred * centred, axis=-1, keepdims=True)
        gain = sm[z, pl.ds(GAIN_ROW, 1), pl.ds(pl.multiple_of(sub * DV, DV), DV)]
        hid[at, :] = (centred * lax.rsqrt(var + epsilon) * gain).astype(BF16)

    lane2 = lax.broadcasted_iota(jnp.int32, (WINDOW, 2 * WINDOW), 1)
    row2 = lax.broadcasted_iota(jnp.int32, (WINDOW, 2 * WINDOW), 0)

    def attention(b):
        at = pl.ds(pl.multiple_of(b * WINDOW, WINDOW), WINDOW)
        band = pl.ds(pl.multiple_of(b * WINDOW, WINDOW), 2 * WINDOW)
        k, v = kv[band, pl.ds(0, HD)], kv[band, pl.ds(128, HD)]
        visible = (lane2 <= row2 + WINDOW) & (lane2 > row2) & (lane2 + b * WINDOW >= WINDOW)
        sinks = sm[z, pl.ds(SINK_ROW, heads_core * groups), pl.ds(0, 128)]
        res = []
        for h in range(groups):
            q = proj[at, pl.ds(h * HD, HD)]
            score = dot_t(q, k) * HD ** (-0.5)
            e = jnp.exp(jnp.where(visible, score, -1e30))
            logit = sinks[h : h + 1, :1]
            for s in range(1, heads_core):
                logit = jnp.where(sub == s, sinks[s * groups + h : s * groups + h + 1, :1], logit)
            sink = jnp.exp(logit)
            total = jnp.sum(e, axis=-1, keepdims=True) + sink
            res.append(dot((e / total).astype(BF16), v))
        hid[at, :] = jnp.concatenate(res, axis=1).astype(BF16)

    def all_weights():
        for kind, cols in ((0, ret_cols), (1, att_cols)):
            @pl.when(c == kind)
            def _():
                for n, (_, _, cd) in enumerate(pieces(0, kind)):
                    arrived(w.at[wrows(z * depth, depth), cd], wsem.at[z, n])
                for i in range(1, n_sp):
                    zs = lax.rem(z + i, n_sp)
                    for k in range(1, n_fs):
                        fs = lax.rem(f + k, n_fs)
                        arrived(w.at[wrows(zs * depth + fs * quarter, quarter), pl.ds(0, cols)],
                                wpsem.at[zs, fs])

    def hand_on(p, cond):
        block = hid.at[pl.ds(pl.multiple_of(p * rows, rows), rows)]
        remote(both(cond, p != z), block, hin.at[c, z], hsem.at[c, z], sp=p)
        local(both(cond, p == z), block, hin.at[c, z], hsem.at[c, z])

    near = jnp.where(z < n_sp // 2, -1, 1)

    def land(d):
        for s in (near, -near):
            zs, to = z + s * d, z - s
            ok = jnp.logical_and(zs >= 0, zs < n_sp)
            onward = jnp.logical_and(ok, jnp.logical_and(to >= 0, to < n_sp))
            zs, to = jnp.clip(zs, 0, n_sp - 1), jnp.clip(to, 0, n_sp - 1)
            block = toks.at[zs, c]
            pl.when(ok)(functools.partial(arrived, block, tsem.at[zs, c]))
            remote(onward, block, block, tsem.at[zs, c], sp=to)
            remote(ok, block, block, tsem.at[zs, c], tp=peer)

    def attend(first, last):
        @pl.loop(first * per, last * per)
        def _(b):
            attention(b)

    def take(d):
        for s in (-1, 1) if d else (0,):
            zs = z + s * d
            ok = jnp.logical_and(zs >= 0, zs < n_sp)
            zs = jnp.clip(zs, 0, n_sp - 1)

            @pl.when(ok)
            def _():
                arrived(toks.at[zs, peer], tsem.at[zs, peer])
                project(zs)

            first = both(ok, both(is1, zs == 0))
            if s > 0:
                pl.when(both(ok, is1))(functools.partial(attend, zs, zs + 1))
                hand_on(zs, both(ok, is1))
            elif s < 0:
                pl.when(both(ok, is1))(
                    functools.partial(attend, zs + jnp.where(zs == 0, 0, 1), zs + 2)
                )
                hand_on(zs + 1, both(ok, is1))
                hand_on(jnp.int32(0), first)
            else:
                pl.when(first)(functools.partial(attend, zs, zs + 1))
                hand_on(jnp.int32(0), first)

    for d in range(1, n_sp - 1):
        land(d)
    arrived(sm.at[z], smsem.at[z])
    for i in range(1, n_sp):
        zs = lax.rem(z + i, n_sp)
        pl.when(is0)(functools.partial(arrived, sm.at[zs, pl.ds(0, SINK_ROW)], smsem.at[zs]))
    inputs[5].wait()
    inputs[6].wait()
    all_weights()
    pass_out(0)
    pass_out(1)
    for d in range(n_sp - 1):
        take(d)
    land(n_sp - 1)
    take(n_sp - 1)

    @pl.when(is0)
    def _():
        arrived(s0, ssem)
        state[...] = s0[...]

    for p in range(n_sp):
        @pl.when(is0)
        def _():
            pl.loop(0, per)(functools.partial(retention, p))

        hand_on(jnp.int32(p), is0)

    width = hin.shape[3]
    for kind in (1, 0):
        for i in range(n_sp):
            zs = lax.rem(z + i, n_sp)
            block = hin.at[kind, zs]
            arrived(block, hsem.at[kind, zs])
            remote(c == kind, block, block, hsem.at[kind, zs], tp=peer)
        for cs in range(2):
            for j in range(fs_core):
                block, sem = out_block(kind, cs, jnp.int32(j))
                passed = both(c == owner, beside == c * fs_core + j) if kind == 0 else both(
                    c != owner, across == c * fs_core + j
                )
                pl.when(jnp.logical_not(passed))(functools.partial(arrived, block, sem))

        @pl.loop(0, out.shape[1] // 256)
        def _(i):
            cols = pl.ds(pl.multiple_of(i * 256, 256), 256)
            acc = total[:, cols] if kind == 0 else None
            for h in range(n_sp):
                term = dot(hin[kind, h], wo[kind, pl.ds(h * width, width), cols])
                acc = term if acc is None else acc + term
            if kind == 0:
                out[:, cols] = acc.astype(BF16)
            else:
                total[:, cols] = acc

    for cond, copy in sent:
        if cond is None:
            copy.wait_send()
        else:
            pl.when(cond)(copy.wait_send)


def layer(mesh, *args):
    (tokens, norm_gain, ret_query, ret_key, ret_value, att_query, att_key, att_value,
     log_decay, start_state, ret_gain, sink_logits, ret_out, att_out) = args
    n_sp, n_fs, n_tp = mesh.shape["sp"], mesh.shape["fs"], mesh.shape["tp"]
    heads = ret_query.shape[1] // DK
    kv_heads = att_key.shape[1] // HD
    rows, half = tokens.shape[1:]
    whole_heads = (
        n_tp == 2 and n_fs == 4 and heads * n_tp == n_sp and kv_heads == heads
        and att_query.shape[1] == ret_query.shape[1]
    )
    if not whole_heads:
        return shards(*args)
    depth = ret_query.shape[0]
    wide = heads * rows
    small = (SINK_ROW + sink_logits.shape[0], wide)
    h = DK // 2
    inverse = np.float32(1.0) / np.float32(10000.0) ** (np.arange(h, dtype=np.float32) / np.float32(h))
    angles = np.arange(n_sp * rows, dtype=np.float32)[:, None] * inverse[None, :]
    cos = jnp.asarray(np.cos(angles), F32)
    sin = jnp.asarray(np.sin(angles), F32)
    length = n_sp * rows
    vm = pl.BlockSpec(memory_space=pltpu.VMEM)
    hbm = pl.BlockSpec(memory_space=pl.ANY)
    dma = pltpu.SemaphoreType.DMA
    res = pl.pallas_call(
        functools.partial(fused, n_sp, n_fs),
        out_shape=jax.ShapeDtypeStruct((rows, half), BF16),
        in_specs=[hbm] * 16,
        out_specs=vm,
        scratch_shapes=[
            pltpu.VMEM((rows, half), BF16),
            pltpu.VMEM((1, norm_gain.shape[0]), F32),
            pltpu.VMEM(small, F32),
            pltpu.VMEM((length, h), F32),
            pltpu.VMEM((length, h), F32),
            pltpu.VMEM((1, ret_gain.shape[0]), F32),
            pltpu.VMEM((heads, rows), F32),
            pltpu.VMEM((1, sink_logits.shape[0]), F32),
            dma((7,)),
            pltpu.VMEM((n_sp, 2, rows, half), BF16),
            pltpu.VMEM((rows, 128), F32),
            pltpu.VMEM((rows, 128), F32),
            pltpu.VMEM((n_sp * depth, 3 * DK), BF16),
            pltpu.VMEM((2, 2 * ret_out.shape[0], n_fs // 2 * ret_out.shape[1]), BF16),
            pltpu.VMEM((n_sp,) + small, F32),
            pltpu.VMEM((DK, DV), F32),
            pltpu.VMEM((length, 3 * DK), BF16),
            pltpu.VMEM((WINDOW + length, 256), BF16),
            pltpu.VMEM((length, DV), BF16),
            pltpu.VMEM((2, n_sp, rows, DV), BF16),
            pltpu.VMEM((DK, DV), F32),
            pltpu.VMEM((rows, half), F32),
            dma((100,)),
            dma((n_sp, 3)),
            dma((n_sp, n_fs)),
            dma((n_sp,)),
            dma,
            dma,
            dma((n_sp, 2)),
            dma((2, 2, n_fs // 2)),
            dma((2, n_sp)),
            dma,
        ],
        compiler_params=pltpu.CompilerParams(
            collective_id=0, has_side_effects=True, vmem_limit_bytes=67043328
        ),
    )(
        tokens[0], norm_gain[None], ret_query, ret_key, ret_value, att_query, att_key, att_value,
        ret_gain[None], log_decay[0], sink_logits[None], start_state[0], ret_out, att_out, cos, sin,
    )
    return res[None]


def solution(mesh):
    placed = (
        P("fs", "sp", "tp"),
        P(),
        P("sp", "tp"),
        P("sp", "tp"),
        P("sp", "tp"),
        P("sp", "tp"),
        P("sp", "tp"),
        P("sp", "tp"),
        P("fs", "tp", "sp"),
        P("fs", "tp", None, None),
        P("tp"),
        P("tp"),
        P("tp", "fs"),
        P("tp", "fs"),
    )
    return jax.shard_map(
        functools.partial(layer, mesh), mesh=mesh, in_specs=placed, out_specs=P("fs", "sp", "tp"), check_vma=False
    )
```

profile of v0, /device:TPU:1, one launch (start us, length us, event | category | flops | bytes accessed | tf_op | source)
XLA Modules:
  0.0 80.6 jit_solution(4024429976778011525)
XLA Ops:
  0.0 78.7 %shard_map.154 = bf16[256,1024]{1,0:T(8,128)(2,1)} custom-call(bf16[256,1024]{1,0:T(8,128)(2,1)} %bitcast.8, f32[1,2048]{1,0:T(1,128)} %bitcast.10, bf16[512,512]{1,0:T(8,128)(2,1)} %rq.1, bf16[512,512]{1,0:T(8,128)(2,1)} %rk.1, bf16[512,512]{1,0:T(8,128)(2,1)} %rv.1, bf16[512,512]{1,0:T(8,128)(2,1)} %aq.1, bf16[512,128]{1,0:T(8,128)(2,1)} %ak.1, ...), custom_call_target="tpu_custom_call" | custom-call | tf_op jit(solution)/shard_map/pallas_call | solution.py:672
  78.7 1.9 %copy.18 = bf16[1,256,1024]{2,1,0:T(8,128)(2,1)} copy(bf16[1,256,1024]{2,1,0:T(8,128)(2,1)} %bitcast.7) | data formatting | bytes 1048576
where the time goes:
time: 80.7 us; the launch traced here: 80.6 us
  Pallas kernels  78.7 us (98%)
  local copies, waits for them, and re-layouts  1.87 us (2%)
    pallas_call x1, Pallas kernels, layer(): pl.pallas_call(functools.partial(fused, n_sp, n_fs), out_shape=jax.ShapeD...  78.7 us
    unnamed x1, local copies, waits for them, and re-layouts  1.87 us

commit v1 on v0

v1 whole, which is shorter than its diff:
```python
import functools

import jax
import jax.numpy as jnp
import numpy as np
from jax import lax
from jax.experimental import pallas as pl
from jax.experimental.pallas import tpu as pltpu
from jax.sharding import PartitionSpec as P

DK = 256
DV = 256
HD = 64
WINDOW = 128
BLOCK = 128


epsilon = 1e-06
exact_result = lax.Precision.HIGHEST


def carried_in(array, axis, combine, identity):
    peers, mine = (lax.axis_size(axis), lax.axis_index(axis))
    everything = jax.tree.map(
        lambda part, kind: lax.all_gather(part.astype(kind), axis),
        array,
        (jnp.bfloat16, jnp.bfloat16),
    )
    start = jax.tree.map(
        lambda part, zero: jnp.broadcast_to(jnp.asarray(zero, part.dtype), part.shape),
        array,
        identity,
    )

    def hop(k, before):
        reached = k < mine
        new = combine(
            before, jax.tree.map(lambda part, own: part[k].astype(own.dtype), everything, array)
        )
        return jax.tree.map(lambda a, b: jnp.where(reached, a, b), new, before)

    return lax.fori_loop(0, peers, hop, start)


def passed_along(block, axis, distance):
    devices = range(lax.axis_size(axis))
    route = [(i - distance, i) for i in devices if i - distance in devices]
    return lax.ppermute(block, axis, route)


def rotate(values, positions):
    half_dim = values.shape[-1] // 2
    inverse = 1.0 / 10000.0 ** (jnp.arange(half_dim, dtype=jnp.float32) / half_dim)
    angles = positions.astype(jnp.float32)[:, None] * inverse[None, :]
    cosine = jnp.cos(angles)[:, None, :]
    sine_table = jnp.sin(angles)[:, None, :]
    front_half = values[..., :half_dim]
    back_half = values[..., half_dim:]
    return jnp.concatenate(
        [
            front_half * cosine - back_half * sine_table,
            front_half * sine_table + back_half * cosine,
        ],
        axis=-1,
    )


def block_step(memory_state, inputs):
    queries, key_matrix_rows, value_matrix_rows, log_rates = inputs
    length_here = log_rates.shape[-1]
    causal = jnp.arange(length_here)[:, None] >= jnp.arange(length_here)[None, :]
    running_totals = jnp.cumsum(log_rates, axis=-1)
    relative = running_totals[:, :, None] - running_totals[:, None, :]
    weight = jnp.where(causal[None], jnp.exp(jnp.where(causal[None], relative, 0.0)), 0.0)
    score_matrix = (
        jnp.einsum("hqd,hkd->hqk", queries, key_matrix_rows, precision=exact_result) * weight
    )
    carried_state = jnp.einsum(
        "hqd,hdv->hqv",
        queries * jnp.exp(running_totals)[:, :, None],
        memory_state,
        precision=exact_result,
    )
    output_rows = (
        jnp.einsum("arf,afu->aru", score_matrix, value_matrix_rows, precision=exact_result)
        + carried_state
    )
    decay_factors = jnp.exp(running_totals[:, -1:] - running_totals)
    memory_state = memory_state * jnp.exp(running_totals[:, -1])[:, None, None] + jnp.einsum(
        "iwj,iwe->ije",
        key_matrix_rows * decay_factors[:, :, None],
        value_matrix_rows,
        precision=exact_result,
    )
    return (memory_state, output_rows)


def chain(earlier, later):
    return (earlier[0] * later[0], earlier[1] * later[0][:, None, None] + later[1])


def shards(
    tokens,
    norm_gain,
    ret_query,
    ret_key,
    ret_value,
    att_query,
    att_key,
    att_value,
    log_decay,
    start_state,
    ret_gain,
    sink_logits,
    ret_out,
    att_out,
):
    gathered = lax.all_gather(tokens[0], "tp", axis=1, tiled=True)
    row_count = gathered.shape[0]
    as_float = gathered.astype(jnp.float32)
    normed = (
        as_float
        * lax.rsqrt(jnp.mean(as_float * as_float, axis=-1, keepdims=True) + epsilon)
        * norm_gain
    ).astype(jnp.bfloat16)
    offset = lax.axis_index("sp") * row_count
    positions = offset + jnp.arange(row_count, dtype=jnp.int32)
    weights = (ret_query, ret_key, ret_value, att_query, att_key, att_value)
    pieces = (
        lax.all_gather(weights[0], "sp", axis=0, tiled=True),
        lax.all_gather(weights[1], "sp", axis=0, tiled=True),
        lax.all_gather(weights[2], "sp", axis=0, tiled=True),
        lax.all_gather(weights[3], "sp", axis=0, tiled=True),
        lax.all_gather(weights[4], "sp", axis=0, tiled=True),
        lax.all_gather(weights[5], "sp", axis=0, tiled=True),
    )
    projected = tuple(
        (jnp.dot(normed, piece, preferred_element_type=jnp.float32) for piece in pieces)
    )
    rounded = tuple((product_f.astype(jnp.bfloat16) for product_f in projected))
    projected = rounded[:3]
    head_count = projected[0].shape[1] // DK
    queries = rotate(projected[0].astype(jnp.float32).reshape(row_count, head_count, DK), positions)
    keys_rot = rotate(
        projected[1].astype(jnp.float32).reshape(row_count, head_count, DK), positions
    ) * DK ** (-0.5)
    values_f = projected[2].astype(jnp.float32).reshape(row_count, head_count, DV)
    log_rates = log_decay[0]
    count = row_count // BLOCK

    def blocked(array):
        return array.reshape(count, BLOCK, head_count, array.shape[-1]).transpose(0, 2, 1, 3)

    rates_blocked = log_rates.reshape(head_count, count, BLOCK).transpose(1, 0, 2)
    local_state, pieces = lax.scan(
        block_step,
        jnp.zeros((head_count, DK, DV), jnp.float32),
        (blocked(queries), blocked(keys_rot), blocked(values_f), rates_blocked),
    )
    local_out = pieces.transpose(0, 2, 1, 3).reshape(row_count, head_count, DV)
    running_totals = jnp.cumsum(log_rates, axis=-1)
    device_decay = jnp.exp(running_totals[:, -1])
    identity = (jnp.ones((head_count,), jnp.float32), jnp.zeros((head_count, DK, DV), jnp.float32))
    prior_decay, prior_state = carried_in((device_decay, local_state), "sp", chain, identity)
    incoming = prior_state + prior_decay[:, None, None] * start_state[0]
    retained = local_out + jnp.einsum(
        "thd,hdv->thv",
        queries * jnp.exp(running_totals).T[:, :, None],
        incoming,
        precision=exact_result,
    )
    centred = retained - jnp.mean(retained, axis=-1, keepdims=True)
    variance = jnp.mean(centred * centred, axis=-1, keepdims=True)
    ret_hidden = (
        (centred * lax.rsqrt(variance + epsilon)).reshape(row_count, head_count * DV) * ret_gain
    ).astype(jnp.bfloat16)
    att_queries, att_keys, att_values = rounded[3:]
    kv_heads = att_keys.shape[1] // HD
    groups = att_queries.shape[1] // HD // kv_heads
    earlier_keys, earlier_values = passed_along(
        (att_keys[row_count - WINDOW :], att_values[row_count - WINDOW :]), "sp", 1
    )
    extended_keys = jnp.concatenate([earlier_keys, att_keys], axis=0)
    extended_values = jnp.concatenate([earlier_values, att_values], axis=0)
    windows = row_count // WINDOW

    def banded(array):
        earlier = array[:row_count].reshape(windows, WINDOW, kv_heads, HD)
        current = array[WINDOW:].reshape(windows, WINDOW, kv_heads, HD)
        return jnp.concatenate([earlier, current], axis=1)

    key_band = banded(extended_keys)
    value_band = banded(extended_values)
    grouped_q = att_queries.reshape(windows, WINDOW, kv_heads, groups, HD)
    score_matrix = jnp.einsum(
        "nqhgd,nkhd->nhgqk", grouped_q, key_band, preferred_element_type=jnp.float32
    ) * HD ** (-0.5)
    query_index = WINDOW + jnp.arange(WINDOW)
    key_index = jnp.arange(2 * WINDOW)
    allowed = (key_index[None, :] <= query_index[:, None]) & (
        query_index[:, None] - key_index[None, :] < WINDOW
    )
    key_place = offset - WINDOW + jnp.arange(windows)[:, None] * WINDOW + key_index[None, :]
    visible = (allowed[None] & (key_place >= 0)[:, None, :])[:, None, None]
    expo = jnp.exp(jnp.where(visible, score_matrix, -1e30))
    summed = jnp.sum(expo, axis=-1, keepdims=True) + jnp.exp(sink_logits).reshape(
        1, kv_heads, groups, 1, 1
    )
    probs = (expo / summed).astype(jnp.bfloat16)
    attended = jnp.einsum(
        "nhgqk,nkhd->nqhgd", probs, value_band, preferred_element_type=jnp.float32
    )
    att_hidden = attended.astype(jnp.bfloat16).reshape(row_count, kv_heads * groups * HD)
    ret_width = ret_hidden.shape[1]
    joined = jnp.concatenate([ret_hidden, att_hidden], axis=1)[None]
    piece = lax.all_gather(joined, "fs", axis=0, tiled=True)
    product = jnp.einsum(
        "srh,hd->srd", piece[:, :, :ret_width], ret_out, preferred_element_type=jnp.float32
    )
    product = product + jnp.einsum(
        "srh,hd->srd", piece[:, :, ret_width:], att_out, preferred_element_type=jnp.float32
    )
    partial_rows = product.astype(jnp.bfloat16)
    regrouped = lax.all_to_all(partial_rows, "fs", split_axis=0, concat_axis=2, tiled=True)
    mixed = lax.psum_scatter(
        regrouped[0].astype(jnp.float32).astype(jnp.bfloat16), "tp", scatter_dimension=1, tiled=True
    )
    return mixed[None]


MESH = pl.DeviceIdType.MESH
F32 = jnp.float32
BF16 = jnp.bfloat16
GAIN_ROW = 0
DECAY_ROW = 1
SINK_ROW = 2
K_AT, V_AT, KV_AT, Q_AT, A_AT = 0, 256, 512, 640, 896


def dot(a, b):
    return jnp.dot(a, b, preferred_element_type=F32)


def dot_t(a, b):
    return lax.dot_general(a, b, (((1,), (1,)), ((), ())), preferred_element_type=F32)


def dot_l(a, b):
    return lax.dot_general(a, b, (((0,), (0,)), ((), ())), preferred_element_type=F32)


def fused(
    tok_in, ngain_in, rq, rk, rv, aq, ak, av, gain_in, decay_in, sink_in, start, ro, ao, cos_in, sin_in, out,
    ngain, gain_v, decay_v, sink_v, ak_v, av_v, cos, sin, insem,
    small, sm, traw, xn, akp, w, wo, s0, local_state, sbuf, states, kbuf, vbuf, qbuf, aqbuf, kvp, inner, hid, hin,
    total, ob,
    send, smsem, tsem, ownsem, zsem, ysem, psem, wosem, ssem, stsem, halosem, hsem, outsem,
):
    z, f, c = lax.axis_index("sp"), lax.axis_index("fs"), lax.axis_index("tp")
    y, x = f // 2, lax.rem(f, 2)
    zh, zb = z // 2, lax.rem(z, 2)
    peer = 1 - c
    fx, fy = 2 * y + 1 - x, 2 * (1 - y) + x
    zp, z2, z3 = z + 1 - 2 * zb, lax.rem(z + 2, 4), 3 - z
    head = 2 * zb + x
    rows, half = tok_in.shape
    depth = rq.shape[0]
    part = depth // 4
    mid = jnp.logical_or(z == 1, z == 2)
    near, far = jnp.where(mid, z3, z2), jnp.where(mid, z2, z3)
    order = (zp, near, far)
    first, second = zh == 0, zh == 1

    loads = [
        (ngain_in, ngain), (gain_in, gain_v), (decay_in, decay_v), (sink_in, sink_v), (ak, ak_v), (av, av_v),
        (cos_in.at[pl.ds(pl.multiple_of(zh * 2 * rows, 2 * rows), 2 * rows)], cos),
        (sin_in.at[pl.ds(pl.multiple_of(zh * 2 * rows, 2 * rows), 2 * rows)], sin),
    ]
    inputs = [pltpu.make_async_copy(src, dst, insem.at[i]) for i, (src, dst) in enumerate(loads)]
    for copy in inputs:
        copy.start()

    barrier = pltpu.get_barrier_semaphore()
    greeted = [{"tp": peer}, {"fs": fy}]
    for t in range(2):
        core = jnp.int32(t)
        greeted += [{"sp": zs, "tp": core} for zs in order]
        greeted += [{"fs": fx, "tp": core}, {"sp": zp, "fs": fx, "tp": core}]
    for where in greeted:
        pl.semaphore_signal(barrier, inc=1, device_id=where, device_id_type=MESH)
    pl.semaphore_wait(barrier, len(greeted))

    sent = []
    slots = iter(range(send.shape[0]))

    def both(a, b):
        if a is None:
            return b
        return a if b is None else jnp.logical_and(a, b)

    def remote(cond, src, dst, rsem, **where):
        copy = pltpu.make_async_remote_copy(
            src_ref=src, dst_ref=dst, send_sem=send.at[next(slots)], recv_sem=rsem,
            device_id=where, device_id_type=MESH,
        )
        sent.append((cond, copy))
        if cond is None:
            copy.start()
        else:
            pl.when(cond)(copy.start)

    def local(cond, src, dst, sem):
        copy = pltpu.make_async_copy(src, dst, sem)
        if cond is None:
            copy.start()
        else:
            pl.when(cond)(copy.start)

    def arrived(dst, sem):
        pltpu.make_async_copy(dst, dst, sem).wait()

    mine = traw.at[zb, c]
    local(c == x, tok_in, mine, tsem.at[zb, c])
    remote(c != x, tok_in, mine, tsem.at[zb, c], tp=peer)
    remote(None, tok_in, mine, tsem.at[zb, c], sp=zp, tp=x)
    remote(None, tok_in, mine, tsem.at[zb, c], fs=fx, tp=x)

    pieces = ((K_AT, 512), (KV_AT, 128), (Q_AT, 256), (A_AT, 256))

    def rows_of(zs, ys, cs):
        return pl.ds(pl.multiple_of(zs * depth + ys * 2 * part + cs * part, part), part)

    to_a = jnp.where(zb == c, z2, zp)
    column = pl.ds(pl.multiple_of(x * DK, DK), DK)

    def send_weights(p):
        arrays = {0: ((rk, K_AT, DK), (rv, V_AT, DK)), 1: ((akp, KV_AT, 128),), 2: ((rq, Q_AT, DK),),
                  3: ((aq, A_AT, DK),)}[p]
        for a, at, width in arrays:
            cols = pl.ds(0, width) if a is akp else column
            for cond, to in ((None, to_a), (zb != c, z3)):
                for t in range(2):
                    src = a.at[pl.ds(pl.multiple_of(y * 2 * part + t * part, part), part), cols]
                    remote(cond, src, w.at[rows_of(z, y, t), pl.ds(at, width)], zsem.at[p, z], sp=to, tp=jnp.int32(t))
        for a, at, width in arrays:
            cols = pl.ds(0, width) if a is akp else column
            dst = w.at[pl.ds(pl.multiple_of(z * depth, depth), depth), pl.ds(at, width)]
            local(c == zb, a.at[:, cols], dst, ownsem.at[p])
            remote(c == zb, a.at[:, cols], dst, ownsem.at[p], tp=peer)

    send_weights(0)

    out_rows, out_cols = ro.shape

    def out_block(kind, ys, cs):
        return wo.at[kind, ys, pl.ds(pl.multiple_of(cs * out_rows, out_rows), out_rows)], wosem.at[kind, ys, cs]

    def send_out(kind):
        a = (ro, ao)[kind]
        block, sem = out_block(kind, y, c)
        remote(None, a, block, sem, fs=fy)
        remote(None, a, block, sem, tp=peer)
        local(None, a, block, sem)

    def pass_out(kind):
        block, sem = out_block(kind, 1 - y, c)
        arrived(block, sem)
        remote(None, block, block, sem, tp=peer)

    def wait_out(kind):
        for ys, cs in ((y, c), (y, peer), (1 - y, peer)):
            arrived(*out_block(kind, ys, cs))

    send_out(0)

    for i in (1, 2, 3):
        inputs[i].wait()
    small[...] = jnp.zeros_like(small)
    small[pl.ds(GAIN_ROW, 1), :] = gain_v[...]
    for j in range(2):
        small[pl.ds(DECAY_ROW, 1), pl.ds(j * rows, rows)] = decay_v[pl.ds(j, 1), :]
    small[pl.ds(SINK_ROW, 1), pl.ds(0, sink_v.shape[1])] = sink_v[...]
    inputs[4].wait()
    inputs[5].wait()
    packed = [
        jnp.concatenate([ak_v[:, j * HD : (j + 1) * HD], av_v[:, j * HD : (j + 1) * HD]], axis=1) for j in range(2)
    ]
    akp[...] = jnp.where(x == 0, packed[0], packed[1])

    for xs in range(2):
        dx = x if xs == 0 else 1 - x
        fd = f if xs == 0 else fx
        here = jnp.logical_and(zb == c, c == x) if xs == 0 else None
        away = jnp.logical_not(here) if xs == 0 else None
        if xs == 0:
            local(here, small, sm.at[zb], smsem.at[zb])
        remote(away, small, sm.at[zb], smsem.at[zb], sp=2 * zh + c, fs=fd, tp=x)
        gives = jnp.logical_and(first, zb == c)
        src = start.at[dx]
        if xs == 0:
            local(both(gives, c == x), src, s0, ssem)
            remote(both(gives, c != x), src, s0, ssem, tp=peer)
        else:
            remote(gives, src, s0, ssem, fs=fd, tp=x)

    send_weights(1)
    send_weights(2)
    send_weights(3)

    for t in range(2):
        block = traw.at[1 - zb, t]

        @pl.when(c == x)
        def _():
            arrived(block, tsem.at[1 - zb, t])

        remote(c == x, block, block, tsem.at[1 - zb, t], fs=fx)

    def take(p):
        at, width = pieces[p]
        cols = pl.ds(at, width)
        for zs in order:
            block = w.at[rows_of(zs, y, c), cols]
            arrived(block, zsem.at[p, zs])
            remote(None, block, block, ysem.at[p, zs], fs=fy)
            remote(None, block, block, psem.at[p], tp=peer)

    def spread(p):
        at, width = pieces[p]
        cols = pl.ds(at, width)
        for zs in order:
            block = w.at[rows_of(zs, 1 - y, c), cols]
            arrived(block, ysem.at[p, zs])
            remote(None, block, block, psem.at[p], tp=peer)

    def complete(p):
        at, width = pieces[p]
        cols = pl.ds(at, width)
        arrived(w.at[pl.ds(0, depth), cols], ownsem.at[p])
        arrived(w.at[pl.ds(0, 6 * part), cols], psem.at[p])

    inputs[0].wait()

    def normalize(b):
        @pl.loop(0, rows // 32)
        def _(i):
            at = pl.ds(pl.multiple_of(i * 32, 32), 32)
            to = pl.ds(pl.multiple_of(b * rows + i * 32, 32), 32)
            h0, h1 = traw[b, 0, at, :].astype(F32), traw[b, 1, at, :].astype(F32)
            squares = jnp.sum(h0 * h0, axis=-1, keepdims=True) + jnp.sum(h1 * h1, axis=-1, keepdims=True)
            scale = lax.rsqrt(squares / (2 * half) + epsilon)
            xn[to, pl.ds(0, half)] = (h0 * scale * ngain[:, pl.ds(0, half)]).astype(BF16)
            xn[to, pl.ds(half, half)] = (h1 * scale * ngain[:, pl.ds(half, half)]).astype(BF16)

    def token_wait(b):
        for t in range(2):
            block, sem = traw.at[b, t], tsem.at[b, t]
            if b is other:
                pl.when(c != x)(functools.partial(arrived, block, sem))
            else:
                arrived(block, sem)

    own, other = zb, 1 - zb
    token_wait(own)
    normalize(own)
    take(0)
    send_out(1)
    spread(0)
    token_wait(other)
    normalize(other)
    inputs[6].wait()
    inputs[7].wait()
    for b in range(2):
        arrived(sm.at[b], smsem.at[b])
    complete(0)

    def block_at(b):
        return pl.ds(pl.multiple_of(b * rows, rows), rows)

    def tile(b, at, width):
        return dot(xn[block_at(b), :], w[:, pl.ds(at, width)])

    h = DK // 2

    def turn(a, b, factor):
        co, si = cos[block_at(b), :], sin[block_at(b), :]
        lo, hi = a[:, :h], a[:, h:]
        return jnp.concatenate([(lo * co - hi * si) * factor, (lo * si + hi * co) * factor], axis=1).astype(BF16)

    lane = lax.broadcasted_iota(jnp.int32, (rows, rows), 1)
    row = lax.broadcasted_iota(jnp.int32, (rows, rows), 0)

    def rates(b):
        l = sm[b, pl.ds(DECAY_ROW, 1), pl.ds(pl.multiple_of(x * rows, rows), rows)]
        cum = jnp.sum(jnp.where(lane <= row, l, 0.0), axis=1, keepdims=True)
        return cum, jnp.sum(l, axis=1, keepdims=True)

    @pl.loop(0, 2)
    def _(b):
        at = block_at(b)
        k = turn(tile(b, K_AT, DK).astype(BF16).astype(F32), b, DK ** (-0.5))
        kbuf[at, :] = k
        v = tile(b, V_AT, DV).astype(BF16)
        vbuf[at, :] = v
        cum, whole = rates(b)
        kd = (k.astype(F32) * jnp.exp(whole - cum)).astype(BF16)
        local_state[b] = dot_l(kd, v)

    def decay_of(b):
        return jnp.exp(rates(b)[1])

    @pl.when(first)
    def _():
        arrived(s0, ssem)
        states[0] = s0[...].astype(BF16)
        after = s0[...] * decay_of(0) + local_state[0]
        states[1] = after.astype(BF16)
        sbuf[...] = (after * decay_of(1) + local_state[1]).astype(BF16)

    remote(first, sbuf, states.at[0], stsem, sp=z2)

    take(1)
    spread(1)
    take(2)
    complete(1)

    @pl.when(first)
    def _():
        kvp[pl.ds(0, WINDOW), :] = jnp.zeros((WINDOW, kvp.shape[1]), BF16)

    @pl.loop(0, 2)
    def _(b):
        to = pl.ds(pl.multiple_of(WINDOW + b * rows, WINDOW), rows)
        kvp[to, :] = tile(b, KV_AT, 128).astype(BF16)

    remote(first, kvp.at[pl.ds(2 * rows, WINDOW)], kvp.at[pl.ds(0, WINDOW)], halosem, sp=z2)
    pass_out(0)
    spread(2)
    take(3)
    complete(2)

    @pl.loop(0, 2)
    def _(b):
        at = block_at(b)
        q = turn(tile(b, Q_AT, DK).astype(BF16).astype(F32), b, 1.0)
        qbuf[at, :] = q
        cum, _ = rates(b)
        cum_row = jnp.sum(jnp.where(lane == row, cum, 0.0), axis=0, keepdims=True)
        weight = jnp.where(lane <= row, jnp.exp(jnp.where(lane <= row, cum - cum_row, 0.0)), 0.0)
        scores = (dot_t(q, kbuf[at, :]) * weight).astype(BF16)
        inner[at, :] = dot(scores, vbuf[at, :])

    spread(3)

    @pl.when(second)
    def _():
        arrived(states.at[0], stsem)
        states[1] = (states[0].astype(F32) * decay_of(0) + local_state[0]).astype(BF16)

    def hand_on(kind, b):
        if b is other:
            remote(None, hid.at[kind, other], hin.at[kind, head], hsem.at[kind, head], sp=zp)
            remote(None, hid.at[kind, other], hin.at[kind, head], hsem.at[kind, head], sp=zp, fs=fx)
        else:
            remote(None, hid.at[kind, own], hin.at[kind, head], hsem.at[kind, head], fs=fx)
            local(None, hid.at[kind, own], hin.at[kind, head], hsem.at[kind, head])

    gain_at = pl.ds(pl.multiple_of(x * DV, DV), DV)
    for b in (other, own):
        at = block_at(b)
        cum, _ = rates(b)
        o = inner[at, :] + dot((qbuf[at, :].astype(F32) * jnp.exp(cum)).astype(BF16), states[b])
        centred = o - jnp.mean(o, axis=-1, keepdims=True)
        var = jnp.mean(centred * centred, axis=-1, keepdims=True)
        hid[0, b] = (centred * lax.rsqrt(var + epsilon) * sm[0, pl.ds(GAIN_ROW, 1), gain_at]).astype(BF16)
        hand_on(0, b)

    complete(3)

    @pl.loop(0, 2)
    def _(b):
        aqbuf[block_at(b), :] = tile(b, A_AT, DK).astype(BF16)

    lane2 = lax.broadcasted_iota(jnp.int32, (WINDOW, 2 * WINDOW), 1)
    row2 = lax.broadcasted_iota(jnp.int32, (WINDOW, 2 * WINDOW), 0)
    per = rows // WINDOW
    groups = DK // HD
    pl.when(second)(functools.partial(arrived, kvp.at[pl.ds(0, WINDOW)], halosem))
    sink_row = sm[0, pl.ds(SINK_ROW, 1), pl.ds(0, 128)]
    sink_lane = lax.broadcasted_iota(jnp.int32, (1, 128), 1)
    sinks = [
        jnp.exp(jnp.sum(jnp.where(sink_lane == x * groups + i, sink_row, 0.0), axis=1, keepdims=True))
        for i in range(groups)
    ]

    for b in (other, own):
        @pl.loop(0, per)
        def _(i):
            n = b * per + i
            at = pl.ds(pl.multiple_of(n * WINDOW, WINDOW), WINDOW)
            band = kvp[pl.ds(pl.multiple_of(n * WINDOW, WINDOW), 2 * WINDOW), :]
            k, v = band[:, :HD], band[:, HD:]
            seen = (lane2 <= row2 + WINDOW) & (lane2 > row2)
            visible = seen & (lane2 + n * WINDOW + zh * 2 * rows >= WINDOW)
            res = []
            for g in range(groups):
                q = aqbuf[at, pl.ds(g * HD, HD)]
                e = jnp.exp(jnp.where(visible, dot_t(q, k) * HD ** (-0.5), -1e30))
                norm = jnp.sum(e, axis=-1, keepdims=True) + sinks[g]
                res.append(dot((e / norm).astype(BF16), v))
            hid[1, b, pl.ds(pl.multiple_of(i * WINDOW, WINDOW), WINDOW), :] = jnp.concatenate(res, axis=1).astype(BF16)

        hand_on(1, b)

    pass_out(1)
    wait_out(0)
    for kind in range(2):
        if kind == 1:
            wait_out(1)
        for hz, hx in ((zb, x), (1 - zb, x), (zb, 1 - x), (1 - zb, 1 - x)):
            arrived(hin.at[kind, 2 * hz + hx], hsem.at[kind, 2 * hz + hx])
        for t in range(4):
            cols = pl.ds(t % 2 * 256, 256)
            acc = None
            for n in range(4):
                term = dot(hin[kind, n], wo[kind, t // 2, pl.ds(n * DV, DV), cols])
                acc = term if acc is None else acc + term
            if kind == 0:
                total[:, pl.ds(t * 256, 256)] = acc
                continue
            ob[t] = (total[:, pl.ds(t * 256, 256)] + acc).astype(BF16)
            yq = t // 2
            dst = out.at[:, pl.ds(pl.multiple_of(x * out_cols + t % 2 * 256, 256), 256)]
            home = c == x
            local(both(home, c == yq), ob.at[t], dst, outsem)
            remote(both(home, c != yq), ob.at[t], dst, outsem, tp=peer)
            remote(jnp.logical_not(home), ob.at[t], dst, outsem, fs=fx, tp=jnp.int32(yq))

    arrived(out, outsem)
    for cond, copy in sent:
        if cond is None:
            copy.wait_send()
        else:
            pl.when(cond)(copy.wait_send)


def layer(mesh, *args):
    (tokens, norm_gain, ret_query, ret_key, ret_value, att_query, att_key, att_value,
     log_decay, start_state, ret_gain, sink_logits, ret_out, att_out) = args
    n_sp, n_fs, n_tp = mesh.shape["sp"], mesh.shape["fs"], mesh.shape["tp"]
    heads = ret_query.shape[1] // DK
    kv_heads = att_key.shape[1] // HD
    rows, half = tokens.shape[1:]
    depth = ret_query.shape[0]
    square = (
        n_tp == 2 and n_fs == 4 and n_sp == 4 and heads == 2 and kv_heads == 2
        and att_query.shape[1] == ret_query.shape[1] and rows == DK and tokens.shape[0] == 1
        and 2 * half == n_sp * depth and ret_out.shape == att_out.shape
        and ret_out.shape == (heads * DV, half // 2) and half == 4 * DK
    )
    if not square:
        return shards(*args)
    h = DK // 2
    length = n_sp * rows
    inverse = np.float32(1.0) / np.float32(10000.0) ** (np.arange(h, dtype=np.float32) / np.float32(h))
    angles = np.arange(length, dtype=np.float32)[:, None] * inverse[None, :]
    cos = jnp.asarray(np.cos(angles), F32)
    sin = jnp.asarray(np.sin(angles), F32)
    wide = heads * rows
    hbm = pl.BlockSpec(memory_space=pl.ANY)
    dma = pltpu.SemaphoreType.DMA
    v = pltpu.VMEM
    res = pl.pallas_call(
        fused,
        out_shape=jax.ShapeDtypeStruct((rows, half), BF16),
        in_specs=[hbm] * 16,
        out_specs=hbm,
        scratch_shapes=[
            v((1, norm_gain.shape[0]), F32),
            v((1, ret_gain.shape[0]), F32),
            v((heads, rows), F32),
            v((1, sink_logits.shape[0]), F32),
            v(att_key.shape, BF16),
            v(att_value.shape, BF16),
            v((2 * rows, h), F32),
            v((2 * rows, h), F32),
            dma((8,)),
            v((8, wide), F32),
            v((2, 8, wide), F32),
            v((2, 2, rows, half), BF16),
            v((2 * rows, 2 * half), BF16),
            v((depth, 128), BF16),
            v((n_sp * depth, A_AT + DK), BF16),
            v((2, 2, 2 * ret_out.shape[0], ret_out.shape[1]), BF16),
            v((DK, DV), F32),
            v((2, DK, DV), F32),
            v((DK, DV), BF16),
            v((2, DK, DV), BF16),
            v((2 * rows, DK), BF16),
            v((2 * rows, DV), BF16),
            v((2 * rows, DK), BF16),
            v((2 * rows, DK), BF16),
            v((WINDOW + 2 * rows, 128), BF16),
            v((2 * rows, DV), F32),
            v((2, 2, rows, DV), BF16),
            v((2, 4, rows, DV), BF16),
            v((rows, half), F32),
            v((4, rows, 256), BF16),
            dma((128,)),
            dma((2,)),
            dma((2, 2)),
            dma((4,)),
            dma((4, n_sp)),
            dma((4, n_sp)),
            dma((4,)),
            dma((2, 2, 2)),
            dma,
            dma,
            dma,
            dma((2, 4)),
            dma,
        ],
        compiler_params=pltpu.CompilerParams(
            collective_id=0, has_side_effects=True, vmem_limit_bytes=67043328
        ),
    )(
        tokens[0], norm_gain[None], ret_query, ret_key, ret_value, att_query, att_key, att_value,
        ret_gain[None], log_decay[0], sink_logits[None], start_state[0], ret_out, att_out, cos, sin,
    )
    return res[None]


def solution(mesh):
    placed = (
        P("fs", "sp", "tp"),
        P(),
        P("sp", "tp"),
        P("sp", "tp"),
        P("sp", "tp"),
        P("sp", "tp"),
        P("sp", "tp"),
        P("sp", "tp"),
        P("fs", "tp", "sp"),
        P("fs", "tp", None, None),
        P("tp"),
        P("tp"),
        P("tp", "fs"),
        P("tp", "fs"),
    )
    return jax.shard_map(
        functools.partial(layer, mesh), mesh=mesh, in_specs=placed, out_specs=P("fs", "sp", "tp"), check_vma=False
    )
```

time: 80.7 us -> 89.5 us (1.11)
  Pallas kernels: 78.7 us -> 87.4 us
    pallas_call x1, Pallas kernels: 78.7 us -> 87.4 us  [layer(): pl.pallas_call(fused, out_shape=jax.ShapeDtypeStruct((rows, half), BF16),...]
where the time goes in v1:
time: 89.5 us; the launch traced here: 89.3 us
  Pallas kernels  87.4 us (98%)
  local copies, waits for them, and re-layouts  1.87 us (2%)
    pallas_call x1, Pallas kernels, layer(): pl.pallas_call(fused, out_shape=jax.ShapeDtypeStruct((rows, half), BF16),...  87.4 us
    unnamed x1, local copies, waits for them, and re-layouts  1.87 us

profile of v1, /device:TPU:1, one launch (start us, length us, event | category | flops | bytes accessed | tf_op | source)
XLA Modules:
  0.0 89.3 jit_solution(9825682039341090326)
XLA Ops:
  0.0 87.4 %shard_map.154 = bf16[256,1024]{1,0:T(8,128)(2,1)} custom-call(bf16[256,1024]{1,0:T(8,128)(2,1)} %bitcast.8, f32[1,2048]{1,0:T(1,128)} %bitcast.10, bf16[512,512]{1,0:T(8,128)(2,1)} %rq.1, bf16[512,512]{1,0:T(8,128)(2,1)} %rk.1, bf16[512,512]{1,0:T(8,128)(2,1)} %rv.1, bf16[512,512]{1,0:T(8,128)(2,1)} %aq.1, bf16[512,128]{1,0:T(8,128)(2,1)} %ak.1, ...), custom_call_target="tpu_custom_call" | custom-call | tf_op jit(solution)/shard_map/pallas_call | solution.py:673
  87.4 1.9 %copy.18 = bf16[1,256,1024]{2,1,0:T(8,128)(2,1)} copy(bf16[1,256,1024]{2,1,0:T(8,128)(2,1)} %bitcast.7) | data formatting | bytes 1048576

commit v2 on v1

--- a/solution.py
+++ b/solution.py
@@ -308,6 +308,7 @@
             copy.start()
         else:
             pl.when(cond)(copy.start)
+        return copy
 
     def local(cond, src, dst, sem):
         copy = pltpu.make_async_copy(src, dst, sem)
@@ -322,56 +323,78 @@
     mine = traw.at[zb, c]
     local(c == x, tok_in, mine, tsem.at[zb, c])
     remote(c != x, tok_in, mine, tsem.at[zb, c], tp=peer)
-    remote(None, tok_in, mine, tsem.at[zb, c], sp=zp, tp=x)
+    ahead = remote(None, tok_in, mine, tsem.at[zb, c], sp=zp, tp=x)
     remote(None, tok_in, mine, tsem.at[zb, c], fs=fx, tp=x)
 
-    pieces = ((K_AT, 512), (KV_AT, 128), (Q_AT, 256), (A_AT, 256))
+    pieces = ((K_AT, DK), (V_AT, DV), (KV_AT, 128), (Q_AT, DK), (A_AT, 128), (A_AT + 128, 128))
+    sources = (rk, rv, akp, rq, aq, aq)
+    halved = 4
 
     def rows_of(zs, ys, cs):
         return pl.ds(pl.multiple_of(zs * depth + ys * 2 * part + cs * part, part), part)
 
+    def rows_whole(zs, cs):
+        return pl.ds(pl.multiple_of(zs * depth + cs * 2 * part, 2 * part), 2 * part)
+
+    def weight(p):
+        a, (at, width) = sources[p], pieces[p]
+        offset = x * DK + (128 if p == 5 else 0)
+        return a, pl.ds(0, width) if a is akp else pl.ds(pl.multiple_of(offset, 128), width), pl.ds(at, width)
+
+    def send_weights(p, cond, to):
+        a, cols, at = weight(p)
+        for t in range(2):
+            if p < halved:
+                src = a.at[pl.ds(pl.multiple_of(y * 2 * part + t * part, part), part), cols]
+                dst = w.at[rows_of(z, y, t), at]
+            else:
+                src = a.at[pl.ds(t * 2 * part, 2 * part), cols]
+                dst = w.at[rows_whole(z, t), at]
+            remote(cond, src, dst, zsem.at[p, z], sp=to, tp=jnp.int32(t))
+
+    def keep_weights(p):
+        a, cols, at = weight(p)
+        dst = w.at[pl.ds(pl.multiple_of(z * depth, depth), depth), at]
+        local(c == zb, a.at[:, cols], dst, ownsem.at[p])
+        remote(c == zb, a.at[:, cols], dst, ownsem.at[p], tp=peer)
+
     to_a = jnp.where(zb == c, z2, zp)
-    column = pl.ds(pl.multiple_of(x * DK, DK), DK)
-
-    def send_weights(p):
-        arrays = {0: ((rk, K_AT, DK), (rv, V_AT, DK)), 1: ((akp, KV_AT, 128),), 2: ((rq, Q_AT, DK),),
-                  3: ((aq, A_AT, DK),)}[p]
-        for a, at, width in arrays:
-            cols = pl.ds(0, width) if a is akp else column
-            for cond, to in ((None, to_a), (zb != c, z3)):
-                for t in range(2):
-                    src = a.at[pl.ds(pl.multiple_of(y * 2 * part + t * part, part), part), cols]
-                    remote(cond, src, w.at[rows_of(z, y, t), pl.ds(at, width)], zsem.at[p, z], sp=to, tp=jnp.int32(t))
-        for a, at, width in arrays:
-            cols = pl.ds(0, width) if a is akp else column
-            dst = w.at[pl.ds(pl.multiple_of(z * depth, depth), depth), pl.ds(at, width)]
-            local(c == zb, a.at[:, cols], dst, ownsem.at[p])
-            remote(c == zb, a.at[:, cols], dst, ownsem.at[p], tp=peer)
-
-    send_weights(0)
+    early = jnp.logical_and(zb != c, mid)
+    late = jnp.logical_and(zb != c, jnp.logical_not(mid))
+    for p in (0, 1, 3, 4, 5):
+        send_weights(p, early, z3)
+    for p in (0, 1, 3, 4, 5):
+        keep_weights(p)
 
     out_rows, out_cols = ro.shape
 
-    def out_block(kind, ys, cs):
-        return wo.at[kind, ys, pl.ds(pl.multiple_of(cs * out_rows, out_rows), out_rows)], wosem.at[kind, ys, cs]
-
-    def send_out(kind):
-        a = (ro, ao)[kind]
-        block, sem = out_block(kind, y, c)
+    shares = ((0, 0, out_rows), (1, 0, out_rows // 2), (1, out_rows // 2, out_rows // 2))
+
+    def out_block(share, ys, cs):
+        kind, at, n = shares[share]
+        rows_at = pl.ds(pl.multiple_of(cs * out_rows + at, n), n)
+        return wo.at[kind, ys, rows_at], wosem.at[share, ys, cs]
+
+    def send_out(share):
+        kind, at, n = shares[share]
+        a = (ro, ao)[kind].at[pl.ds(at, n)]
+        block, sem = out_block(share, y, c)
         remote(None, a, block, sem, fs=fy)
         remote(None, a, block, sem, tp=peer)
         local(None, a, block, sem)
 
-    def pass_out(kind):
-        block, sem = out_block(kind, 1 - y, c)
+    def pass_out(share):
+        block, sem = out_block(share, 1 - y, c)
         arrived(block, sem)
         remote(None, block, block, sem, tp=peer)
 
     def wait_out(kind):
-        for ys, cs in ((y, c), (y, peer), (1 - y, peer)):
-            arrived(*out_block(kind, ys, cs))
+        for share in ((0,), (1, 2))[kind]:
+            for ys, cs in ((y, c), (y, peer), (1 - y, peer)):
+                arrived(*out_block(share, ys, cs))
 
     send_out(0)
+    send_out(1)
 
     for i in (1, 2, 3):
         inputs[i].wait()
@@ -387,25 +410,21 @@
     ]
     akp[...] = jnp.where(x == 0, packed[0], packed[1])
 
-    for xs in range(2):
-        dx = x if xs == 0 else 1 - x
-        fd = f if xs == 0 else fx
-        here = jnp.logical_and(zb == c, c == x) if xs == 0 else None
-        away = jnp.logical_not(here) if xs == 0 else None
-        if xs == 0:
-            local(here, small, sm.at[zb], smsem.at[zb])
-        remote(away, small, sm.at[zb], smsem.at[zb], sp=2 * zh + c, fs=fd, tp=x)
-        gives = jnp.logical_and(first, zb == c)
-        src = start.at[dx]
-        if xs == 0:
-            local(both(gives, c == x), src, s0, ssem)
-            remote(both(gives, c != x), src, s0, ssem, tp=peer)
-        else:
-            remote(gives, src, s0, ssem, fs=fd, tp=x)
-
-    send_weights(1)
-    send_weights(2)
-    send_weights(3)
+    send_weights(2, early, z3)
+    keep_weights(2)
+    here = jnp.logical_and(zb == c, c == x)
+    to_square = 2 * zh + c
+    local(here, small, sm.at[zb], smsem.at[zb])
+    remote(jnp.logical_not(here), small, sm.at[zb], smsem.at[zb], sp=to_square, tp=x)
+    remote(None, small, sm.at[zb], smsem.at[zb], sp=to_square, fs=fx, tp=x)
+    gives = jnp.logical_and(first, zb == c)
+    local(both(gives, c == x), start.at[x], s0, ssem)
+    remote(both(gives, c != x), start.at[x], s0, ssem, tp=peer)
+
+    ahead.wait_send()
+    for p in range(len(pieces)):
+        send_weights(p, None, to_a)
+        send_weights(p, late, z3)
 
     for t in range(2):
         block = traw.at[1 - zb, t]
@@ -415,14 +434,17 @@
             arrived(block, tsem.at[1 - zb, t])
 
         remote(c == x, block, block, tsem.at[1 - zb, t], fs=fx)
+
+    remote(gives, start.at[1 - x], s0, ssem, fs=fx, tp=x)
 
     def take(p):
         at, width = pieces[p]
         cols = pl.ds(at, width)
         for zs in order:
-            block = w.at[rows_of(zs, y, c), cols]
+            block = w.at[rows_of(zs, y, c) if p < halved else rows_whole(zs, c), cols]
             arrived(block, zsem.at[p, zs])
-            remote(None, block, block, ysem.at[p, zs], fs=fy)
+            if p < halved:
+                remote(None, block, block, ysem.at[p, zs], fs=fy)
             remote(None, block, block, psem.at[p], tp=peer)
 
     def spread(p):
@@ -464,8 +486,12 @@
     token_wait(own)
     normalize(own)
     take(0)
-    send_out(1)
+    take(1)
     spread(0)
+    take(2)
+    spread(1)
+    take(3)
+    send_out(2)
     token_wait(other)
     normalize(other)
     inputs[6].wait()
@@ -473,6 +499,7 @@
     for b in range(2):
         arrived(sm.at[b], smsem.at[b])
     complete(0)
+    complete(1)
 
     def block_at(b):
         return pl.ds(pl.multiple_of(b * rows, rows), rows)
@@ -519,10 +546,12 @@
 
     remote(first, sbuf, states.at[0], stsem, sp=z2)
 
-    take(1)
-    spread(1)
-    take(2)
-    complete(1)
+    spread(2)
+    spread(3)
+    pass_out(0)
+    pass_out(1)
+    take(4)
+    complete(2)
 
     @pl.when(first)
     def _():
@@ -534,10 +563,18 @@
         kvp[to, :] = tile(b, KV_AT, 128).astype(BF16)
 
     remote(first, kvp.at[pl.ds(2 * rows, WINDOW)], kvp.at[pl.ds(0, WINDOW)], halosem, sp=z2)
-    pass_out(0)
-    spread(2)
-    take(3)
-    complete(2)
+    complete(3)
+
+    def hand_on(kind, b, cols=None):
+        sem = kind if cols is None else kind + cols
+        at = pl.ds(0, DV) if cols is None else pl.ds(cols * 128, 128)
+        src, dst, sem = hid.at[kind, b, :, at], hin.at[kind, head, :, at], hsem.at[sem, head]
+        if b is other:
+            remote(None, src, dst, sem, sp=zp)
+            remote(None, src, dst, sem, sp=zp, fs=fx)
+        else:
+            remote(None, src, dst, sem, fs=fx)
+            local(None, src, dst, sem)
 
     @pl.loop(0, 2)
     def _(b):
@@ -550,20 +587,10 @@
         scores = (dot_t(q, kbuf[at, :]) * weight).astype(BF16)
         inner[at, :] = dot(scores, vbuf[at, :])
 
-    spread(3)
-
     @pl.when(second)
     def _():
         arrived(states.at[0], stsem)
         states[1] = (states[0].astype(F32) * decay_of(0) + local_state[0]).astype(BF16)
-
-    def hand_on(kind, b):
-        if b is other:
-            remote(None, hid.at[kind, other], hin.at[kind, head], hsem.at[kind, head], sp=zp)
-            remote(None, hid.at[kind, other], hin.at[kind, head], hsem.at[kind, head], sp=zp, fs=fx)
-        else:
-            remote(None, hid.at[kind, own], hin.at[kind, head], hsem.at[kind, head], fs=fx)
-            local(None, hid.at[kind, own], hin.at[kind, head], hsem.at[kind, head])
 
     gain_at = pl.ds(pl.multiple_of(x * DV, DV), DV)
     for b in (other, own):
@@ -574,12 +601,6 @@
         var = jnp.mean(centred * centred, axis=-1, keepdims=True)
         hid[0, b] = (centred * lax.rsqrt(var + epsilon) * sm[0, pl.ds(GAIN_ROW, 1), gain_at]).astype(BF16)
         hand_on(0, b)
-
-    complete(3)
-
-    @pl.loop(0, 2)
-    def _(b):
-        aqbuf[block_at(b), :] = tile(b, A_AT, DK).astype(BF16)
 
     lane2 = lax.broadcasted_iota(jnp.int32, (WINDOW, 2 * WINDOW), 1)
     row2 = lax.broadcasted_iota(jnp.int32, (WINDOW, 2 * WINDOW), 0)
@@ -593,32 +614,44 @@
         for i in range(groups)
     ]
 
-    for b in (other, own):
-        @pl.loop(0, per)
-        def _(i):
+    take(5)
+    def attend(part_at, b):
+        cols = pl.ds(part_at * 128, 128)
+        aqbuf[block_at(b), cols] = tile(b, A_AT + part_at * 128, 128).astype(BF16)
+        for i in range(per):
             n = b * per + i
             at = pl.ds(pl.multiple_of(n * WINDOW, WINDOW), WINDOW)
             band = kvp[pl.ds(pl.multiple_of(n * WINDOW, WINDOW), 2 * WINDOW), :]
             k, v = band[:, :HD], band[:, HD:]
             seen = (lane2 <= row2 + WINDOW) & (lane2 > row2)
             visible = seen & (lane2 + n * WINDOW + zh * 2 * rows >= WINDOW)
-            res = []
-            for g in range(groups):
-                q = aqbuf[at, pl.ds(g * HD, HD)]
-                e = jnp.exp(jnp.where(visible, dot_t(q, k) * HD ** (-0.5), -1e30))
-                norm = jnp.sum(e, axis=-1, keepdims=True) + sinks[g]
-                res.append(dot((e / norm).astype(BF16), v))
-            hid[1, b, pl.ds(pl.multiple_of(i * WINDOW, WINDOW), WINDOW), :] = jnp.concatenate(res, axis=1).astype(BF16)
-
-        hand_on(1, b)
-
-    pass_out(1)
-    wait_out(0)
+            q = aqbuf[at, cols]
+            score = dot_t(jnp.concatenate([q[:, :HD], q[:, HD:]], axis=0), k) * HD ** (-0.5)
+            probs = []
+            for g in range(2):
+                e = jnp.exp(jnp.where(visible, score[g * WINDOW : (g + 1) * WINDOW], -1e30))
+                norm = 1.0 / (jnp.sum(e, axis=-1, keepdims=True) + sinks[part_at * 2 + g])
+                probs.append((e * norm).astype(BF16))
+            res = dot(jnp.concatenate(probs, axis=0), v)
+            to = pl.ds(i * WINDOW, WINDOW)
+            hid[1, b, to, cols] = jnp.concatenate([res[:WINDOW], res[WINDOW:]], axis=1).astype(BF16)
+
+    for part_at in range(2):
+        complete(4 + part_at)
+        for b in (other, own):
+            attend(part_at, b)
+            hand_on(1, b, part_at)
+
+    pass_out(2)
     for kind in range(2):
-        if kind == 1:
-            wait_out(1)
+        wait_out(kind)
         for hz, hx in ((zb, x), (1 - zb, x), (zb, 1 - x), (1 - zb, 1 - x)):
-            arrived(hin.at[kind, 2 * hz + hx], hsem.at[kind, 2 * hz + hx])
+            n = 2 * hz + hx
+            if kind == 0:
+                arrived(hin.at[0, n], hsem.at[0, n])
+            else:
+                for i in range(2):
+                    arrived(hin.at[1, n, :, pl.ds(i * 128, 128)], hsem.at[1 + i, n])
         for t in range(4):
             cols = pl.ds(t % 2 * 256, 256)
             acc = None
@@ -638,6 +671,8 @@
 
     arrived(out, outsem)
     for cond, copy in sent:
+        if copy is ahead:
+            continue
         if cond is None:
             copy.wait_send()
         else:
@@ -709,15 +744,15 @@
             dma((128,)),
             dma((2,)),
             dma((2, 2)),
-            dma((4,)),
-            dma((4, n_sp)),
-            dma((4, n_sp)),
-            dma((4,)),
-            dma((2, 2, 2)),
+            dma((6,)),
+            dma((6, n_sp)),
+            dma((6, n_sp)),
+            dma((6,)),
+            dma((3, 2, 2)),
             dma,
             dma,
             dma,
-            dma((2, 4)),
+            dma((3, 4)),
             dma,
         ],
         compiler_params=pltpu.CompilerParams(

time: 89.5 us -> 73.1 us (0.82)
  the two profiles are of different devices: /device:TPU:1 before, /device:TPU:17 now
where the time goes in v2:
time: 73.1 us; the launch traced here: 73 us
  Pallas kernels  71.1 us (97%)
  local copies, waits for them, and re-layouts  1.87 us (3%)
    pallas_call x1, Pallas kernels, layer(): pl.pallas_call(fused, out_shape=jax.ShapeDtypeStruct((rows, half), BF16),...  71.1 us
    unnamed x1, local copies, waits for them, and re-layouts  1.87 us

profile of v2, /device:TPU:17, one launch (start us, length us, event | category | flops | bytes accessed | tf_op | source)
XLA Modules:
  0.0 73.0 jit_solution(9584341548759376517)
XLA Ops:
  0.0 71.1 %shard_map.154 = bf16[256,1024]{1,0:T(8,128)(2,1)} custom-call(bf16[256,1024]{1,0:T(8,128)(2,1)} %bitcast.8, f32[1,2048]{1,0:T(1,128)} %bitcast.10, bf16[512,512]{1,0:T(8,128)(2,1)} %rq.1, bf16[512,512]{1,0:T(8,128)(2,1)} %rk.1, bf16[512,512]{1,0:T(8,128)(2,1)} %rv.1, bf16[512,512]{1,0:T(8,128)(2,1)} %aq.1, bf16[512,128]{1,0:T(8,128)(2,1)} %ak.1, ...), custom_call_target="tpu_custom_call" | custom-call | tf_op jit(solution)/shard_map/pallas_call | solution.py:708
  71.1 1.9 %copy.18 = bf16[1,256,1024]{2,1,0:T(8,128)(2,1)} copy(bf16[1,256,1024]{2,1,0:T(8,128)(2,1)} %bitcast.7) | data formatting | bytes 1048576

commit v3 on v2

--- a/solution.py
+++ b/solution.py
@@ -252,8 +252,8 @@
 def fused(
     tok_in, ngain_in, rq, rk, rv, aq, ak, av, gain_in, decay_in, sink_in, start, ro, ao, cos_in, sin_in, out,
     ngain, gain_v, decay_v, sink_v, ak_v, av_v, cos, sin, insem,
-    small, sm, traw, xn, akp, w, wo, s0, local_state, sbuf, states, kbuf, vbuf, qbuf, aqbuf, kvp, inner, hid, hin,
-    total, ob,
+    small, sm, traw, xn, akp, w, wo, s0, local_state, sbuf, states, kbuf, vbuf, qbuf, kvp, inner, hid, hin,
+    total, ob, fade, since, until,
     send, smsem, tsem, ownsem, zsem, ysem, psem, wosem, ssem, stsem, halosem, hsem, outsem,
 ):
     z, f, c = lax.axis_index("sp"), lax.axis_index("fs"), lax.axis_index("tp")
@@ -326,9 +326,9 @@
     ahead = remote(None, tok_in, mine, tsem.at[zb, c], sp=zp, tp=x)
     remote(None, tok_in, mine, tsem.at[zb, c], fs=fx, tp=x)
 
-    pieces = ((K_AT, DK), (V_AT, DV), (KV_AT, 128), (Q_AT, DK), (A_AT, 128), (A_AT + 128, 128))
-    sources = (rk, rv, akp, rq, aq, aq)
-    halved = 4
+    pieces = ((K_AT, DK), (V_AT, DV), (KV_AT, 128), (A_AT, DK), (Q_AT, DK))
+    sources = (rk, rv, akp, aq, rq)
+    whole = (4,)
 
     def rows_of(zs, ys, cs):
         return pl.ds(pl.multiple_of(zs * depth + ys * 2 * part + cs * part, part), part)
@@ -338,18 +338,17 @@
 
     def weight(p):
         a, (at, width) = sources[p], pieces[p]
-        offset = x * DK + (128 if p == 5 else 0)
-        return a, pl.ds(0, width) if a is akp else pl.ds(pl.multiple_of(offset, 128), width), pl.ds(at, width)
+        return a, pl.ds(0, width) if a is akp else pl.ds(pl.multiple_of(x * DK, DK), width), pl.ds(at, width)
 
     def send_weights(p, cond, to):
         a, cols, at = weight(p)
         for t in range(2):
-            if p < halved:
+            if p in whole:
+                src = a.at[pl.ds(t * 2 * part, 2 * part), cols]
+                dst = w.at[rows_whole(z, t), at]
+            else:
                 src = a.at[pl.ds(pl.multiple_of(y * 2 * part + t * part, part), part), cols]
                 dst = w.at[rows_of(z, y, t), at]
-            else:
-                src = a.at[pl.ds(t * 2 * part, 2 * part), cols]
-                dst = w.at[rows_whole(z, t), at]
             remote(cond, src, dst, zsem.at[p, z], sp=to, tp=jnp.int32(t))
 
     def keep_weights(p):
@@ -361,9 +360,9 @@
     to_a = jnp.where(zb == c, z2, zp)
     early = jnp.logical_and(zb != c, mid)
     late = jnp.logical_and(zb != c, jnp.logical_not(mid))
-    for p in (0, 1, 3, 4, 5):
+    for p in (0, 1, 3, 4):
         send_weights(p, early, z3)
-    for p in (0, 1, 3, 4, 5):
+    for p in (0, 1, 3, 4):
         keep_weights(p)
 
     out_rows, out_cols = ro.shape
@@ -422,7 +421,7 @@
     remote(both(gives, c != x), start.at[x], s0, ssem, tp=peer)
 
     ahead.wait_send()
-    for p in range(len(pieces)):
+    for p in (2, 0, 1, 3, 4):
         send_weights(p, None, to_a)
         send_weights(p, late, z3)
 
@@ -441,9 +440,9 @@
         at, width = pieces[p]
         cols = pl.ds(at, width)
         for zs in order:
-            block = w.at[rows_of(zs, y, c) if p < halved else rows_whole(zs, c), cols]
+            block = w.at[rows_whole(zs, c) if p in whole else rows_of(zs, y, c), cols]
             arrived(block, zsem.at[p, zs])
-            if p < halved:
+            if p not in whole:
                 remote(None, block, block, ysem.at[p, zs], fs=fy)
             remote(None, block, block, psem.at[p], tp=peer)
 
@@ -485,21 +484,40 @@
     own, other = zb, 1 - zb
     token_wait(own)
     normalize(own)
+    pl.when(c == x)(functools.partial(normalize, other))
+    for b in range(2):
+        arrived(sm.at[b], smsem.at[b])
+    lane = lax.broadcasted_iota(jnp.int32, (rows, rows), 1)
+    row = lax.broadcasted_iota(jnp.int32, (rows, rows), 0)
+
+    def rates(b):
+        return sm[b, pl.ds(DECAY_ROW, 1), pl.ds(pl.multiple_of(x * rows, rows), rows)]
+
+    @pl.loop(0, 2)
+    def _(b):
+        at = pl.ds(pl.multiple_of(b * rows, rows), rows)
+        l = rates(b)
+        cum = jnp.sum(jnp.where(lane <= row, l, 0.0), axis=1, keepdims=True)
+        cum_row = jnp.sum(jnp.where(lane == row, cum, 0.0), axis=0, keepdims=True)
+        fade[b] = jnp.where(lane <= row, jnp.exp(jnp.where(lane <= row, cum - cum_row, 0.0)), 0.0)
+        since[at, :] = jnp.exp(cum)
+        until[at, :] = jnp.exp(jnp.sum(l, axis=1, keepdims=True) - cum)
+
+    pass_out(0)
+    take(2)
     take(0)
+    spread(2)
     take(1)
+    pass_out(1)
     spread(0)
-    take(2)
     spread(1)
     take(3)
     send_out(2)
     token_wait(other)
-    normalize(other)
+    pl.when(c != x)(functools.partial(normalize, other))
     inputs[6].wait()
     inputs[7].wait()
-    for b in range(2):
-        arrived(sm.at[b], smsem.at[b])
-    complete(0)
-    complete(1)
+    complete(2)
 
     def block_at(b):
         return pl.ds(pl.multiple_of(b * rows, rows), rows)
@@ -514,14 +532,18 @@
         lo, hi = a[:, :h], a[:, h:]
         return jnp.concatenate([(lo * co - hi * si) * factor, (lo * si + hi * co) * factor], axis=1).astype(BF16)
 
-    lane = lax.broadcasted_iota(jnp.int32, (rows, rows), 1)
-    row = lax.broadcasted_iota(jnp.int32, (rows, rows), 0)
-
-    def rates(b):
-        l = sm[b, pl.ds(DECAY_ROW, 1), pl.ds(pl.multiple_of(x * rows, rows), rows)]
-        cum = jnp.sum(jnp.where(lane <= row, l, 0.0), axis=1, keepdims=True)
-        return cum, jnp.sum(l, axis=1, keepdims=True)
-
+    @pl.when(first)
+    def _():
+        kvp[pl.ds(0, WINDOW), :] = jnp.zeros((WINDOW, kvp.shape[1]), BF16)
+
+    @pl.loop(0, 2)
+    def _(b):
+        to = pl.ds(pl.multiple_of(WINDOW + b * rows, WINDOW), rows)
+        kvp[to, :] = tile(b, KV_AT, 128).astype(BF16)
+
+    remote(first, kvp.at[pl.ds(2 * rows, WINDOW)], kvp.at[pl.ds(0, WINDOW)], halosem, sp=z2)
+    complete(0)
+    complete(1)
     @pl.loop(0, 2)
     def _(b):
         at = block_at(b)
@@ -529,12 +551,11 @@
         kbuf[at, :] = k
         v = tile(b, V_AT, DV).astype(BF16)
         vbuf[at, :] = v
-        cum, whole = rates(b)
-        kd = (k.astype(F32) * jnp.exp(whole - cum)).astype(BF16)
+        kd = (k.astype(F32) * until[at, :]).astype(BF16)
         local_state[b] = dot_l(kd, v)
 
     def decay_of(b):
-        return jnp.exp(rates(b)[1])
+        return jnp.exp(jnp.sum(rates(b), axis=1, keepdims=True))
 
     @pl.when(first)
     def _():
@@ -546,67 +567,22 @@
 
     remote(first, sbuf, states.at[0], stsem, sp=z2)
 
-    spread(2)
-    spread(3)
-    pass_out(0)
-    pass_out(1)
-    take(4)
-    complete(2)
-
-    @pl.when(first)
-    def _():
-        kvp[pl.ds(0, WINDOW), :] = jnp.zeros((WINDOW, kvp.shape[1]), BF16)
-
-    @pl.loop(0, 2)
-    def _(b):
-        to = pl.ds(pl.multiple_of(WINDOW + b * rows, WINDOW), rows)
-        kvp[to, :] = tile(b, KV_AT, 128).astype(BF16)
-
-    remote(first, kvp.at[pl.ds(2 * rows, WINDOW)], kvp.at[pl.ds(0, WINDOW)], halosem, sp=z2)
-    complete(3)
-
-    def hand_on(kind, b, cols=None):
-        sem = kind if cols is None else kind + cols
-        at = pl.ds(0, DV) if cols is None else pl.ds(cols * 128, 128)
-        src, dst, sem = hid.at[kind, b, :, at], hin.at[kind, head, :, at], hsem.at[sem, head]
-        if b is other:
-            remote(None, src, dst, sem, sp=zp)
-            remote(None, src, dst, sem, sp=zp, fs=fx)
-        else:
-            remote(None, src, dst, sem, fs=fx)
-            local(None, src, dst, sem)
-
-    @pl.loop(0, 2)
-    def _(b):
-        at = block_at(b)
-        q = turn(tile(b, Q_AT, DK).astype(BF16).astype(F32), b, 1.0)
-        qbuf[at, :] = q
-        cum, _ = rates(b)
-        cum_row = jnp.sum(jnp.where(lane == row, cum, 0.0), axis=0, keepdims=True)
-        weight = jnp.where(lane <= row, jnp.exp(jnp.where(lane <= row, cum - cum_row, 0.0)), 0.0)
-        scores = (dot_t(q, kbuf[at, :]) * weight).astype(BF16)
-        inner[at, :] = dot(scores, vbuf[at, :])
-
-    @pl.when(second)
-    def _():
-        arrived(states.at[0], stsem)
-        states[1] = (states[0].astype(F32) * decay_of(0) + local_state[0]).astype(BF16)
-
-    gain_at = pl.ds(pl.multiple_of(x * DV, DV), DV)
-    for b in (other, own):
-        at = block_at(b)
-        cum, _ = rates(b)
-        o = inner[at, :] + dot((qbuf[at, :].astype(F32) * jnp.exp(cum)).astype(BF16), states[b])
-        centred = o - jnp.mean(o, axis=-1, keepdims=True)
-        var = jnp.mean(centred * centred, axis=-1, keepdims=True)
-        hid[0, b] = (centred * lax.rsqrt(var + epsilon) * sm[0, pl.ds(GAIN_ROW, 1), gain_at]).astype(BF16)
-        hand_on(0, b)
+    def hand_on(kind, b, away=None, part_at=None):
+        at = pl.ds(0, rows) if part_at is None else pl.ds(part_at * (rows // 2), rows // 2)
+        sem = hsem.at[2 if kind else part_at, head]
+        src, dst = hid.at[kind, b, at], hin.at[kind, head, at]
+        leaves, stays = (zb != b, zb == b) if away is None else (None, None)
+        if away is not False:
+            remote(leaves, src, dst, sem, sp=zp)
+            remote(leaves, src, dst, sem, sp=zp, fs=fx)
+        if away is not True:
+            remote(stays, src, dst, sem, fs=fx)
+            local(stays, src, dst, sem)
 
     lane2 = lax.broadcasted_iota(jnp.int32, (WINDOW, 2 * WINDOW), 1)
     row2 = lax.broadcasted_iota(jnp.int32, (WINDOW, 2 * WINDOW), 0)
     per = rows // WINDOW
     groups = DK // HD
-    pl.when(second)(functools.partial(arrived, kvp.at[pl.ds(0, WINDOW)], halosem))
     sink_row = sm[0, pl.ds(SINK_ROW, 1), pl.ds(0, 128)]
     sink_lane = lax.broadcasted_iota(jnp.int32, (1, 128), 1)
     sinks = [
@@ -614,60 +590,103 @@
         for i in range(groups)
     ]
 
-    take(5)
-    def attend(part_at, b):
-        cols = pl.ds(part_at * 128, 128)
-        aqbuf[block_at(b), cols] = tile(b, A_AT + part_at * 128, 128).astype(BF16)
+    def attention(b, away):
+        aqs = tile(b, A_AT, DK).astype(BF16)
+        seen = (lane2 <= row2 + WINDOW) & (lane2 > row2)
+        scores, bands = [], []
         for i in range(per):
             n = b * per + i
-            at = pl.ds(pl.multiple_of(n * WINDOW, WINDOW), WINDOW)
             band = kvp[pl.ds(pl.multiple_of(n * WINDOW, WINDOW), 2 * WINDOW), :]
-            k, v = band[:, :HD], band[:, HD:]
-            seen = (lane2 <= row2 + WINDOW) & (lane2 > row2)
-            visible = seen & (lane2 + n * WINDOW + zh * 2 * rows >= WINDOW)
-            q = aqbuf[at, cols]
-            score = dot_t(jnp.concatenate([q[:, :HD], q[:, HD:]], axis=0), k) * HD ** (-0.5)
+            bands.append(band[:, HD:])
+            q = aqs[i * WINDOW : (i + 1) * WINDOW]
+            stacked = jnp.concatenate([q[:, g * HD : (g + 1) * HD] for g in range(groups)], axis=0)
+            scores.append(dot_t(stacked, band[:, :HD]))
+        weights = []
+        for i in range(per):
+            visible = seen & (lane2 + (b * per + i) * WINDOW + zh * 2 * rows >= WINDOW)
             probs = []
-            for g in range(2):
-                e = jnp.exp(jnp.where(visible, score[g * WINDOW : (g + 1) * WINDOW], -1e30))
-                norm = 1.0 / (jnp.sum(e, axis=-1, keepdims=True) + sinks[part_at * 2 + g])
-                probs.append((e * norm).astype(BF16))
-            res = dot(jnp.concatenate(probs, axis=0), v)
-            to = pl.ds(i * WINDOW, WINDOW)
-            hid[1, b, to, cols] = jnp.concatenate([res[:WINDOW], res[WINDOW:]], axis=1).astype(BF16)
+            for g in range(groups):
+                part_score = scores[i][g * WINDOW : (g + 1) * WINDOW] * HD ** (-0.5)
+                e = jnp.exp(jnp.where(visible, part_score, -1e30))
+                probs.append((e * (1.0 / (jnp.sum(e, axis=-1, keepdims=True) + sinks[g]))).astype(BF16))
+            weights.append(jnp.concatenate(probs, axis=0))
+        for i in range(per):
+            res = dot(weights[i], bands[i])
+            heads_out = [res[g * WINDOW : (g + 1) * WINDOW] for g in range(groups)]
+            hid[1, b, pl.ds(i * WINDOW, WINDOW), :] = jnp.concatenate(heads_out, axis=1).astype(BF16)
+        hand_on(1, b, away)
+
+    spread(3)
+    complete(3)
+    pl.when(second)(functools.partial(arrived, kvp.at[pl.ds(0, WINDOW)], halosem))
+    attention(other, True)
+    take(4)
+    attention(own, False)
+    complete(4)
+
+    @pl.loop(0, 2)
+    def _(b):
+        at = block_at(b)
+        q = turn(tile(b, Q_AT, DK).astype(BF16).astype(F32), b, 1.0)
+        qbuf[at, :] = (q.astype(F32) * since[at, :]).astype(BF16)
+        scores = (dot_t(q, kbuf[at, :]) * fade[b]).astype(BF16)
+        inner[at, :] = dot(scores, vbuf[at, :])
+
+    @pl.when(second)
+    def _():
+        arrived(states.at[0], stsem)
+        states[1] = (states[0].astype(F32) * decay_of(0) + local_state[0]).astype(BF16)
+
+    gain_at = pl.ds(pl.multiple_of(x * DV, DV), DV)
+    for b in (other, own):
+        at = block_at(b)
+        o = inner[at, :] + dot(qbuf[at, :], states[b])
+        centred = o - jnp.mean(o, axis=-1, keepdims=True)
+        var = jnp.mean(centred * centred, axis=-1, keepdims=True)
+        hid[0, b] = (centred * lax.rsqrt(var + epsilon) * sm[0, pl.ds(GAIN_ROW, 1), gain_at]).astype(BF16)
 
     for part_at in range(2):
-        complete(4 + part_at)
-        for b in (other, own):
-            attend(part_at, b)
-            hand_on(1, b, part_at)
+        hand_on(0, other, True, part_at)
+        hand_on(0, own, False, part_at)
 
     pass_out(2)
-    for kind in range(2):
-        wait_out(kind)
-        for hz, hx in ((zb, x), (1 - zb, x), (zb, 1 - x), (1 - zb, 1 - x)):
-            n = 2 * hz + hx
-            if kind == 0:
-                arrived(hin.at[0, n], hsem.at[0, n])
-            else:
-                for i in range(2):
-                    arrived(hin.at[1, n, :, pl.ds(i * 128, 128)], hsem.at[1 + i, n])
+    others = (2 * zb + 1 - x, 2 * (1 - zb) + x, 2 * (1 - zb) + 1 - x)
+    home = c == x
+
+    def mixed_tile(kind, at, t):
+        cols = pl.ds(t % 2 * 256, 256)
+        acc = None
+        for n in range(4):
+            term = dot(hin[kind, n, at, :], wo[kind, t // 2, pl.ds(n * DV, DV), cols])
+            acc = term if acc is None else acc + term
+        return acc
+
+    for n in (head,) + others:
+        arrived(hin.at[1, n], hsem.at[2, n])
+    wait_out(1)
+    wait_out(0)
+    for t in range(4):
+        total[:, pl.ds(t * 256, 256)] = mixed_tile(1, pl.ds(0, rows), t)
+
+    def finish(part_at):
+        at = pl.ds(part_at * (rows // 2), rows // 2)
         for t in range(4):
-            cols = pl.ds(t % 2 * 256, 256)
-            acc = None
-            for n in range(4):
-                term = dot(hin[kind, n], wo[kind, t // 2, pl.ds(n * DV, DV), cols])
-                acc = term if acc is None else acc + term
-            if kind == 0:
-                total[:, pl.ds(t * 256, 256)] = acc
-                continue
-            ob[t] = (total[:, pl.ds(t * 256, 256)] + acc).astype(BF16)
-            yq = t // 2
-            dst = out.at[:, pl.ds(pl.multiple_of(x * out_cols + t % 2 * 256, 256), 256)]
-            home = c == x
-            local(both(home, c == yq), ob.at[t], dst, outsem)
-            remote(both(home, c != yq), ob.at[t], dst, outsem, tp=peer)
-            remote(jnp.logical_not(home), ob.at[t], dst, outsem, fs=fx, tp=jnp.int32(yq))
+            ob[t, at, :] = (total[at, pl.ds(t * 256, 256)] + mixed_tile(0, at, t)).astype(BF16)
+            src = ob.at[t, at]
+            dst = out.at[at, pl.ds(pl.multiple_of(x * out_cols + t % 2 * 256, 256), 256)]
+            local(both(home, c == t // 2), src, dst, outsem)
+            remote(both(home, c != t // 2), src, dst, outsem, tp=peer)
+            remote(jnp.logical_not(home), src, dst, outsem, fs=fx, tp=jnp.int32(t // 2))
+
+    def wait_ret(part_at):
+        at = pl.ds(part_at * (rows // 2), rows // 2)
+        for n in (head,) + others:
+            arrived(hin.at[0, n, at], hsem.at[part_at, n])
+
+    wait_ret(0)
+    finish(0)
+    wait_ret(1)
+    finish(1)
 
     arrived(out, outsem)
     for cond, copy in sent:
@@ -734,20 +753,22 @@
             v((2 * rows, DK), BF16),
             v((2 * rows, DV), BF16),
             v((2 * rows, DK), BF16),
-            v((2 * rows, DK), BF16),
             v((WINDOW + 2 * rows, 128), BF16),
             v((2 * rows, DV), F32),
             v((2, 2, rows, DV), BF16),
             v((2, 4, rows, DV), BF16),
             v((rows, half), F32),
             v((4, rows, 256), BF16),
-            dma((128,)),
+            v((2, rows, rows), F32),
+            v((2 * rows, 1), F32),
+            v((2 * rows, 1), F32),
+            dma((160,)),
             dma((2,)),
             dma((2, 2)),
-            dma((6,)),
-            dma((6, n_sp)),
-            dma((6, n_sp)),
-            dma((6,)),
+            dma((5,)),
+            dma((5, n_sp)),
+            dma((5, n_sp)),
+            dma((5,)),
             dma((3, 2, 2)),
             dma,
             dma,

time: 73.1 us -> 70.4 us (0.963)
  the two profiles are of different devices: /device:TPU:17 before, /device:TPU:1 now
where the time goes in v3:
time: 70.4 us; the launch traced here: 70.2 us
  Pallas kernels  68.4 us (97%)
  local copies, waits for them, and re-layouts  1.87 us (3%)
    pallas_call x1, Pallas kernels, layer(): pl.pallas_call(fused, out_shape=jax.ShapeDtypeStruct((rows, half), BF16),...  68.4 us
    unnamed x1, local copies, waits for them, and re-layouts  1.87 us

profile of v3, /device:TPU:1, one launch (start us, length us, event | category | flops | bytes accessed | tf_op | source)
XLA Modules:
  0.0 70.2 jit_solution(14653835998190070730)
XLA Ops:
  0.0 68.4 %shard_map.154 = bf16[256,1024]{1,0:T(8,128)(2,1)} custom-call(bf16[256,1024]{1,0:T(8,128)(2,1)} %bitcast.8, f32[1,2048]{1,0:T(1,128)} %bitcast.10, bf16[512,512]{1,0:T(8,128)(2,1)} %rq.1, bf16[512,512]{1,0:T(8,128)(2,1)} %rk.1, bf16[512,512]{1,0:T(8,128)(2,1)} %rv.1, bf16[512,512]{1,0:T(8,128)(2,1)} %aq.1, bf16[512,128]{1,0:T(8,128)(2,1)} %ak.1, ...), custom_call_target="tpu_custom_call" | custom-call | tf_op jit(solution)/shard_map/pallas_call | solution.py:727
  68.4 1.9 %copy.18 = bf16[1,256,1024]{2,1,0:T(8,128)(2,1)} copy(bf16[1,256,1024]{2,1,0:T(8,128)(2,1)} %bitcast.7) | data formatting | bytes 1048576

commit v4 on v3

--- a/solution.py
+++ b/solution.py
@@ -421,9 +421,13 @@
     remote(both(gives, c != x), start.at[x], s0, ssem, tp=peer)
 
     ahead.wait_send()
-    for p in (2, 0, 1, 3, 4):
+
+    def send_rest(p):
         send_weights(p, None, to_a)
         send_weights(p, late, z3)
+
+    for p in (2, 0, 1):
+        send_rest(p)
 
     for t in range(2):
         block = traw.at[1 - zb, t]
@@ -506,12 +510,14 @@
     pass_out(0)
     take(2)
     take(0)
+    send_rest(3)
     spread(2)
     take(1)
+    send_rest(4)
     pass_out(1)
     spread(0)
+    take(3)
     spread(1)
-    take(3)
     send_out(2)
     token_wait(other)
     pl.when(c != x)(functools.partial(normalize, other))
@@ -536,7 +542,7 @@
     def _():
         kvp[pl.ds(0, WINDOW), :] = jnp.zeros((WINDOW, kvp.shape[1]), BF16)
 
-    @pl.loop(0, 2)
+    @pl.loop(0, 2, unroll=True)
     def _(b):
         to = pl.ds(pl.multiple_of(WINDOW + b * rows, WINDOW), rows)
         kvp[to, :] = tile(b, KV_AT, 128).astype(BF16)
@@ -544,7 +550,7 @@
     remote(first, kvp.at[pl.ds(2 * rows, WINDOW)], kvp.at[pl.ds(0, WINDOW)], halosem, sp=z2)
     complete(0)
     complete(1)
-    @pl.loop(0, 2)
+    @pl.loop(0, 2, unroll=True)
     def _(b):
         at = block_at(b)
         k = turn(tile(b, K_AT, DK).astype(BF16).astype(F32), b, DK ** (-0.5))
@@ -624,7 +630,7 @@
     attention(own, False)
     complete(4)
 
-    @pl.loop(0, 2)
+    @pl.loop(0, 2, unroll=True)
     def _(b):
         at = block_at(b)
         q = turn(tile(b, Q_AT, DK).astype(BF16).astype(F32), b, 1.0)

time: 70.4 us -> 68.9 us (0.979)
  Pallas kernels: 68.4 us -> 66.9 us
    pallas_call x1, Pallas kernels: 68.4 us -> 66.9 us  [layer(): pl.pallas_call(fused, out_shape=jax.ShapeDtypeStruct((rows, half), BF16),...]
where the time goes in v4:
time: 68.9 us; the launch traced here: 68.8 us
  Pallas kernels  66.9 us (97%)
  local copies, waits for them, and re-layouts  1.87 us (3%)
    pallas_call x1, Pallas kernels, layer(): pl.pallas_call(fused, out_shape=jax.ShapeDtypeStruct((rows, half), BF16),...  66.9 us
    unnamed x1, local copies, waits for them, and re-layouts  1.87 us

profile of v4, /device:TPU:1, one launch (start us, length us, event | category | flops | bytes accessed | tf_op | source)
XLA Modules:
  0.0 68.8 jit_solution(15892122824204469460)
XLA Ops:
  0.0 66.9 %shard_map.154 = bf16[256,1024]{1,0:T(8,128)(2,1)} custom-call(bf16[256,1024]{1,0:T(8,128)(2,1)} %bitcast.8, f32[1,2048]{1,0:T(1,128)} %bitcast.10, bf16[512,512]{1,0:T(8,128)(2,1)} %rq.1, bf16[512,512]{1,0:T(8,128)(2,1)} %rk.1, bf16[512,512]{1,0:T(8,128)(2,1)} %rv.1, bf16[512,512]{1,0:T(8,128)(2,1)} %aq.1, bf16[512,128]{1,0:T(8,128)(2,1)} %ak.1, ...), custom_call_target="tpu_custom_call" | custom-call | tf_op jit(solution)/shard_map/pallas_call | solution.py:733
  66.9 1.9 %copy.18 = bf16[1,256,1024]{2,1,0:T(8,128)(2,1)} copy(bf16[1,256,1024]{2,1,0:T(8,128)(2,1)} %bitcast.7) | data formatting | bytes 1048576

commit v5 on v4

--- a/solution.py
+++ b/solution.py
@@ -253,8 +253,8 @@
     tok_in, ngain_in, rq, rk, rv, aq, ak, av, gain_in, decay_in, sink_in, start, ro, ao, cos_in, sin_in, out,
     ngain, gain_v, decay_v, sink_v, ak_v, av_v, cos, sin, insem,
     small, sm, traw, xn, akp, w, wo, s0, local_state, sbuf, states, kbuf, vbuf, qbuf, kvp, inner, hid, hin,
-    total, ob, fade, since, until,
-    send, smsem, tsem, ownsem, zsem, ysem, psem, wosem, ssem, stsem, halosem, hsem, outsem,
+    total, ob, fade, since, until, wx,
+    send, smsem, tsem, ownsem, zsem, ysem, psem, wosem, ssem, stsem, halosem, hsem, outsem, xsem,
 ):
     z, f, c = lax.axis_index("sp"), lax.axis_index("fs"), lax.axis_index("tp")
     y, x = f // 2, lax.rem(f, 2)
@@ -392,6 +392,16 @@
             for ys, cs in ((y, c), (y, peer), (1 - y, peer)):
                 arrived(*out_block(share, ys, cs))
 
+    extra_cols = pl.ds(out_cols // 2, out_cols // 2)
+
+    def extra(kind, cs):
+        return wx.at[kind, pl.ds(pl.multiple_of(cs * out_rows, out_rows), out_rows)], xsem.at[kind, cs]
+
+    def send_extra(cond):
+        for kind, a in ((0, ro), (1, ao)):
+            dst, sem = extra(kind, c)
+            remote(cond, a.at[:, extra_cols], dst, sem, fs=fx, tp=1 - x)
+
     send_out(0)
     send_out(1)
 
@@ -489,6 +499,7 @@
     token_wait(own)
     normalize(own)
     pl.when(c == x)(functools.partial(normalize, other))
+    send_extra(c == x)
     for b in range(2):
         arrived(sm.at[b], smsem.at[b])
     lane = lax.broadcasted_iota(jnp.int32, (rows, rows), 1)
@@ -521,6 +532,7 @@
     send_out(2)
     token_wait(other)
     pl.when(c != x)(functools.partial(normalize, other))
+    send_extra(c != x)
     inputs[6].wait()
     inputs[7].wait()
     complete(2)
@@ -667,12 +679,26 @@
             acc = term if acc is None else acc + term
         return acc
 
+    def extra_tile(kind, at):
+        acc = None
+        for n in range(4):
+            term = dot(hin[kind, n, at, :], wx[kind, pl.ds(n * DV, DV), :])
+            acc = term if acc is None else acc + term
+        return acc
+
     for n in (head,) + others:
         arrived(hin.at[1, n], hsem.at[2, n])
     wait_out(1)
     wait_out(0)
     for t in range(4):
         total[:, pl.ds(t * 256, 256)] = mixed_tile(1, pl.ds(0, rows), t)
+
+    @pl.when(home)
+    def _():
+        for kind in range(2):
+            for cs in range(2):
+                arrived(*extra(kind, cs))
+        total[:, pl.ds(half, 256)] = extra_tile(1, pl.ds(0, rows))
 
     def finish(part_at):
         at = pl.ds(part_at * (rows // 2), rows // 2)
@@ -682,7 +708,17 @@
             dst = out.at[at, pl.ds(pl.multiple_of(x * out_cols + t % 2 * 256, 256), 256)]
             local(both(home, c == t // 2), src, dst, outsem)
             remote(both(home, c != t // 2), src, dst, outsem, tp=peer)
-            remote(jnp.logical_not(home), src, dst, outsem, fs=fx, tp=jnp.int32(t // 2))
+            leaves = c != x if t % 2 == 0 else jnp.logical_and(c != x, y != t // 2)
+            remote(leaves, src, dst, outsem, fs=fx, tp=jnp.int32(t // 2))
+
+        @pl.when(home)
+        def _():
+            ob[4, at, :] = (total[at, pl.ds(half, 256)] + extra_tile(0, at)).astype(BF16)
+
+        src = ob.at[4, at]
+        dst = out.at[at, pl.ds(pl.multiple_of((1 - x) * out_cols + out_cols // 2, 256), 256)]
+        local(both(home, c == y), src, dst, outsem)
+        remote(both(home, c != y), src, dst, outsem, tp=peer)
 
     def wait_ret(part_at):
         at = pl.ds(part_at * (rows // 2), rows // 2)
@@ -763,11 +799,12 @@
             v((2 * rows, DV), F32),
             v((2, 2, rows, DV), BF16),
             v((2, 4, rows, DV), BF16),
-            v((rows, half), F32),
-            v((4, rows, 256), BF16),
+            v((rows, half + 256), F32),
+            v((5, rows, 256), BF16),
             v((2, rows, rows), F32),
             v((2 * rows, 1), F32),
             v((2 * rows, 1), F32),
+            v((2, 2 * ret_out.shape[0], ret_out.shape[1] // 2), BF16),
             dma((160,)),
             dma((2,)),
             dma((2, 2)),
@@ -781,6 +818,7 @@
             dma,
             dma((3, 4)),
             dma,
+            dma((2, 2)),
         ],
         compiler_params=pltpu.CompilerParams(
             collective_id=0, has_side_effects=True, vmem_limit_bytes=67043328

time: 68.9 us -> 67.6 us (0.981)
  Pallas kernels: 66.9 us -> 65.5 us
    pallas_call x1, Pallas kernels: 66.9 us -> 65.5 us  [layer(): pl.pallas_call(fused, out_shape=jax.ShapeDtypeStruct((rows, half), BF16),...]
where the time goes in v5:
time: 67.6 us; the launch traced here: 67.4 us
  Pallas kernels  65.5 us (97%)
  local copies, waits for them, and re-layouts  1.87 us (3%)
    pallas_call x1, Pallas kernels, layer(): pl.pallas_call(fused, out_shape=jax.ShapeDtypeStruct((rows, half), BF16),...  65.5 us
    unnamed x1, local copies, waits for them, and re-layouts  1.87 us

profile of v5, /device:TPU:1, one launch (start us, length us, event | category | flops | bytes accessed | tf_op | source)
XLA Modules:
  0.0 67.4 jit_solution(2951675840688814408)
XLA Ops:
  0.0 65.5 %shard_map.154 = bf16[256,1024]{1,0:T(8,128)(2,1)} custom-call(bf16[256,1024]{1,0:T(8,128)(2,1)} %bitcast.8, f32[1,2048]{1,0:T(1,128)} %bitcast.10, bf16[512,512]{1,0:T(8,128)(2,1)} %rq.1, bf16[512,512]{1,0:T(8,128)(2,1)} %rk.1, bf16[512,512]{1,0:T(8,128)(2,1)} %rv.1, bf16[512,512]{1,0:T(8,128)(2,1)} %aq.1, bf16[512,128]{1,0:T(8,128)(2,1)} %ak.1, ...), custom_call_target="tpu_custom_call" | custom-call | tf_op jit(solution)/shard_map/pallas_call | solution.py:769
  65.5 1.9 %copy.18 = bf16[1,256,1024]{2,1,0:T(8,128)(2,1)} copy(bf16[1,256,1024]{2,1,0:T(8,128)(2,1)} %bitcast.7) | data formatting | bytes 1048576

commit v6 on v5

--- a/solution.py
+++ b/solution.py
@@ -251,7 +251,7 @@
 
 def fused(
     tok_in, ngain_in, rq, rk, rv, aq, ak, av, gain_in, decay_in, sink_in, start, ro, ao, cos_in, sin_in, out,
-    ngain, gain_v, decay_v, sink_v, ak_v, av_v, cos, sin, insem,
+    ngain, gain_v, decay_v, sink_v, ak_v, av_v, cos, sin, start_v, start_b, insem,
     small, sm, traw, xn, akp, w, wo, s0, local_state, sbuf, states, kbuf, vbuf, qbuf, kvp, inner, hid, hin,
     total, ob, fade, since, until, wx,
     send, smsem, tsem, ownsem, zsem, ysem, psem, wosem, ssem, stsem, halosem, hsem, outsem, xsem,
@@ -275,6 +275,7 @@
         (ngain_in, ngain), (gain_in, gain_v), (decay_in, decay_v), (sink_in, sink_v), (ak, ak_v), (av, av_v),
         (cos_in.at[pl.ds(pl.multiple_of(zh * 2 * rows, 2 * rows), 2 * rows)], cos),
         (sin_in.at[pl.ds(pl.multiple_of(zh * 2 * rows, 2 * rows), 2 * rows)], sin),
+        (start, start_v),
     ]
     inputs = [pltpu.make_async_copy(src, dst, insem.at[i]) for i, (src, dst) in enumerate(loads)]
     for copy in inputs:
@@ -427,8 +428,10 @@
     remote(jnp.logical_not(here), small, sm.at[zb], smsem.at[zb], sp=to_square, tp=x)
     remote(None, small, sm.at[zb], smsem.at[zb], sp=to_square, fs=fx, tp=x)
     gives = jnp.logical_and(first, zb == c)
-    local(both(gives, c == x), start.at[x], s0, ssem)
-    remote(both(gives, c != x), start.at[x], s0, ssem, tp=peer)
+    inputs[8].wait()
+    start_b[...] = start_v[...].astype(BF16)
+    local(both(gives, c == x), start_b.at[x], s0, ssem)
+    remote(both(gives, c != x), start_b.at[x], s0, ssem, tp=peer)
 
     ahead.wait_send()
 
@@ -448,7 +451,7 @@
 
         remote(c == x, block, block, tsem.at[1 - zb, t], fs=fx)
 
-    remote(gives, start.at[1 - x], s0, ssem, fs=fx, tp=x)
+    remote(gives, start_b.at[1 - x], s0, ssem, fs=fx, tp=x)
 
     def take(p):
         at, width = pieces[p]
@@ -477,7 +480,7 @@
     inputs[0].wait()
 
     def normalize(b):
-        @pl.loop(0, rows // 32)
+        @pl.loop(0, rows // 32, unroll=2)
         def _(i):
             at = pl.ds(pl.multiple_of(i * 32, 32), 32)
             to = pl.ds(pl.multiple_of(b * rows + i * 32, 32), 32)
@@ -578,8 +581,8 @@
     @pl.when(first)
     def _():
         arrived(s0, ssem)
-        states[0] = s0[...].astype(BF16)
-        after = s0[...] * decay_of(0) + local_state[0]
+        states[0] = s0[...]
+        after = s0[...].astype(F32) * decay_of(0) + local_state[0]
         states[1] = after.astype(BF16)
         sbuf[...] = (after * decay_of(1) + local_state[1]).astype(BF16)
 
@@ -637,9 +640,9 @@
     spread(3)
     complete(3)
     pl.when(second)(functools.partial(arrived, kvp.at[pl.ds(0, WINDOW)], halosem))
+    attention(own, False)
     attention(other, True)
     take(4)
-    attention(own, False)
     complete(4)
 
     @pl.loop(0, 2, unroll=True)
@@ -780,7 +783,9 @@
             v(att_value.shape, BF16),
             v((2 * rows, h), F32),
             v((2 * rows, h), F32),
-            dma((8,)),
+            v(start_state.shape[1:], F32),
+            v(start_state.shape[1:], BF16),
+            dma((9,)),
             v((8, wide), F32),
             v((2, 8, wide), F32),
             v((2, 2, rows, half), BF16),
@@ -788,7 +793,7 @@
             v((depth, 128), BF16),
             v((n_sp * depth, A_AT + DK), BF16),
             v((2, 2, 2 * ret_out.shape[0], ret_out.shape[1]), BF16),
-            v((DK, DV), F32),
+            v((DK, DV), BF16),
             v((2, DK, DV), F32),
             v((DK, DV), BF16),
             v((2, DK, DV), BF16),

time: 67.6 us -> 67.4 us (level); the launches traced: 67.4 us -> 66.1 us
  Pallas kernels: 65.5 us -> 64.2 us
    pallas_call x1, Pallas kernels: 65.5 us -> 64.2 us  [layer(): pl.pallas_call(fused, out_shape=jax.ShapeDtypeStruct((rows, half), BF16),...]
where the time goes in v6:
time: 67.4 us; the launch traced here: 66.1 us
  Pallas kernels  64.2 us (95%)
  local copies, waits for them, and re-layouts  1.87 us (3%)
    pallas_call x1, Pallas kernels, layer(): pl.pallas_call(fused, out_shape=jax.ShapeDtypeStruct((rows, half), BF16),...  64.2 us
    unnamed x1, local copies, waits for them, and re-layouts  1.87 us

profile of v6, /device:TPU:1, one launch (start us, length us, event | category | flops | bytes accessed | tf_op | source)
XLA Modules:
  0.0 66.1 jit_solution(5383322666046371298)
XLA Ops:
  0.0 64.2 %shard_map.154 = bf16[256,1024]{1,0:T(8,128)(2,1)} custom-call(bf16[256,1024]{1,0:T(8,128)(2,1)} %bitcast.8, f32[1,2048]{1,0:T(1,128)} %bitcast.10, bf16[512,512]{1,0:T(8,128)(2,1)} %rq.1, bf16[512,512]{1,0:T(8,128)(2,1)} %rk.1, bf16[512,512]{1,0:T(8,128)(2,1)} %rv.1, bf16[512,512]{1,0:T(8,128)(2,1)} %aq.1, bf16[512,128]{1,0:T(8,128)(2,1)} %ak.1, ...), custom_call_target="tpu_custom_call" | custom-call | tf_op jit(solution)/shard_map/pallas_call | solution.py:772
  64.2 1.9 %copy.18 = bf16[1,256,1024]{2,1,0:T(8,128)(2,1)} copy(bf16[1,256,1024]{2,1,0:T(8,128)(2,1)} %bitcast.7) | data formatting | bytes 1048576

commit v7 on v6

--- a/solution.py
+++ b/solution.py
@@ -706,7 +706,12 @@
     def finish(part_at):
         at = pl.ds(part_at * (rows // 2), rows // 2)
         for t in range(4):
-            ob[t, at, :] = (total[at, pl.ds(t * 256, 256)] + mixed_tile(0, at, t)).astype(BF16)
+            needed = True if t % 2 == 0 else jnp.logical_or(home, y != t // 2)
+
+            @pl.when(needed)
+            def _():
+                ob[t, at, :] = (total[at, pl.ds(t * 256, 256)] + mixed_tile(0, at, t)).astype(BF16)
+
             src = ob.at[t, at]
             dst = out.at[at, pl.ds(pl.multiple_of(x * out_cols + t % 2 * 256, 256), 256)]
             local(both(home, c == t // 2), src, dst, outsem)

time: 67.4 us -> 67.3 us (level)
  no operation moved by 1% of the time
where the time goes in v7:
time: 67.3 us; the launch traced here: 66.1 us
  Pallas kernels  64.2 us (95%)
  local copies, waits for them, and re-layouts  1.87 us (3%)
    pallas_call x1, Pallas kernels, layer(): pl.pallas_call(fused, out_shape=jax.ShapeDtypeStruct((rows, half), BF16),...  64.2 us
    unnamed x1, local copies, waits for them, and re-layouts  1.87 us

profile of v7, /device:TPU:1, one launch (start us, length us, event | category | flops | bytes accessed | tf_op | source)
XLA Modules:
  0.0 66.1 jit_solution(8795402816181541480)
XLA Ops:
  0.0 64.2 %shard_map.154 = bf16[256,1024]{1,0:T(8,128)(2,1)} custom-call(bf16[256,1024]{1,0:T(8,128)(2,1)} %bitcast.8, f32[1,2048]{1,0:T(1,128)} %bitcast.10, bf16[512,512]{1,0:T(8,128)(2,1)} %rq.1, bf16[512,512]{1,0:T(8,128)(2,1)} %rk.1, bf16[512,512]{1,0:T(8,128)(2,1)} %rv.1, bf16[512,512]{1,0:T(8,128)(2,1)} %aq.1, bf16[512,128]{1,0:T(8,128)(2,1)} %ak.1, ...), custom_call_target="tpu_custom_call" | custom-call | tf_op jit(solution)/shard_map/pallas_call | solution.py:777
  64.2 1.9 %copy.18 = bf16[1,256,1024]{2,1,0:T(8,128)(2,1)} copy(bf16[1,256,1024]{2,1,0:T(8,128)(2,1)} %bitcast.7) | data formatting | bytes 1048576
